TPU v7x, 256 devices: a whole 4x4x8 slice. The times are simulated.
256 devices in a mesh: sp: 32 (over z, y), tp: 8 (over x, core).
Axes of the slice: x: 4, y: 4, z: 8, core: 2. Of those that a mesh axis runs over, the one named last changes fastest.
Arguments:
- tokens: bfloat16 [16384, 2048], P(('sp', 'tp')), may hold values from -8 to 8, as said below
- w_query: bfloat16 [2048, 1024], P(None, 'tp'), may hold values from -0.125 to 0.125
- w_key: bfloat16 [2048, 1024], P(None, 'tp'), may hold values from -0.125 to 0.125
- w_value: bfloat16 [2048, 1024], P(None, 'tp'), may hold values from -0.125 to 0.125
- head_bias: float32 [16], P('tp'), may hold values from -40 to -3
- w_out: bfloat16 [1024, 2048], P('tp'), may hold values from -0.1875 to 0.1875
Outputs:
- mixed: bfloat16 [16384, 2048], P(('sp', 'tp'))
Inputs may be any that keep to these rules, and one draw needn't show every extreme that they name: `tokens`: activations of order one whose mean shifts between blocks of 512 positions.
All inputs are finite; a program needn't handle non-finite values.
Results may differ from a plain program's by a relative error of at most 0.014.
Values may be sent and summed in bfloat16 or wider, within the bound.
A program may use at most 128 MiB of HBM per device.

v0:
```python
import jax
import jax.numpy as jnp
from jax import lax
from jax.sharding import PartitionSpec as P


def copy_for_each(x, axis):
    copies = jnp.broadcast_to(x, (lax.axis_size(axis), *x.shape))
    return lax.all_to_all(copies, axis, split_axis=0, concat_axis=0, tiled=True)


def in_order(blocks, dim):
    blocks = jnp.moveaxis(blocks, 0, dim)
    lengths = blocks.shape
    return blocks.reshape(*lengths[:dim], lengths[dim] * lengths[dim + 1], *lengths[dim + 2 :])


def gather_directly(x, axis, dim):
    blocks = copy_for_each(x, axis)
    return in_order(blocks, dim)


def in_one_piece(arrays, axis, dim, along):
    widths = [a.shape[along] for a in arrays]
    both = jnp.concatenate(arrays, axis=along)
    out = lax.all_gather(both, axis, axis=dim, tiled=True)
    return tuple(jnp.split(out, [sum(widths[:k]) for k in range(1, len(widths))], axis=along))


def cut_along(x, dim, devices):
    before, after = (x.shape[:dim], x.shape[dim + 1 :])
    return jnp.moveaxis(x.reshape(*before, devices, -1, *after), dim, 0)


def sum_at_owner(x, axis, dim):
    devices = lax.axis_size(axis)
    blocks = lax.all_to_all(cut_along(x, dim, devices), axis, 0, 0, tiled=True)
    return jnp.sum(blocks.astype(jnp.float32), axis=0)


def segment_terms(query_rows, query_pos, key_span, value_span, key_pos, bias):
    head_size = query_rows.shape[2]
    scores = jnp.einsum("rhd,sthd->rhst", query_rows, key_span, preferred_element_type=jnp.float32)
    scores = scores * head_size ** (-0.5) + bias[None, :, None, None]
    causal = key_pos[None, None] < query_pos[:, None, None, None]
    log_keep = jnp.where(causal, jax.nn.log_sigmoid(-scores), 0.0)
    tail = lax.cumsum(log_keep, axis=3, reverse=True) - log_keep
    weights = jnp.where(causal, jnp.exp(jax.nn.log_sigmoid(scores) + tail), 0.0).astype(
        jnp.bfloat16
    )
    segment_out = jnp.einsum(
        "rhst,sthd->rhsd", weights, value_span, preferred_element_type=jnp.float32
    )
    segment_total = jnp.sum(log_keep, axis=3)
    return (segment_out, segment_total)


def span_attention(
    query_rows, query_pos, key_all, value_all, bias, span_segments, segment_rows, block_count
):
    row_total, heads_here, head_size = query_rows.shape
    span_length = span_segments * segment_rows
    key_blocks = key_all.reshape(-1, span_segments, segment_rows, heads_here, head_size)
    value_blocks = value_all.reshape(-1, span_segments, segment_rows, heads_here, head_size)

    def turn(step_index, running):
        accumulated, carried = running
        block_index = block_count - 1 - step_index
        key_span = lax.dynamic_index_in_dim(key_blocks, block_index, 0, keepdims=False)
        value_span = lax.dynamic_index_in_dim(value_blocks, block_index, 0, keepdims=False)
        key_pos = block_index * span_length + jnp.arange(span_length, dtype=jnp.int32).reshape(
            span_segments, segment_rows
        )
        segment_out, segment_total = segment_terms(
            query_rows, query_pos, key_span, value_span, key_pos, bias
        )
        later = lax.cumsum(segment_total, axis=2, reverse=True) - segment_total
        factor = jnp.exp(carried[..., None] + later)
        accumulated = accumulated + jnp.sum(factor[..., None] * segment_out, axis=2)
        carried = carried + jnp.sum(segment_total, axis=2)
        return (accumulated, carried)

    start_state = (
        jnp.zeros((row_total, heads_here, head_size), jnp.float32),
        jnp.zeros((row_total, heads_here), jnp.float32),
    )
    return lax.fori_loop(0, block_count, turn, start_state)[0]


def shards(tokens, w_query, w_key, w_value, head_bias, w_out):
    local_width = w_query.shape[1]
    heads_here = head_bias.shape[0]
    head_size = local_width // heads_here
    joined = jnp.concatenate([w_query, w_key, w_value], axis=1)
    projected = jnp.dot(
        gather_directly(tokens, "tp", 0), joined, preferred_element_type=jnp.float32
    ).astype(jnp.bfloat16)
    own_rows = projected.shape[0]
    queries = projected[:, :local_width]
    keys_local = projected[:, local_width : 2 * local_width]
    values_local = projected[:, 2 * local_width :]
    seq_count = lax.axis_size("sp")
    seq_index = lax.axis_index("sp")
    span_segments = max(
        (
            divisor
            for divisor in range(1, seq_count + 1)
            if seq_count % divisor == 0 and divisor * own_rows <= max(1024, own_rows)
        )
    )
    span_length = span_segments * own_rows
    query_heads = queries.reshape(own_rows, heads_here, head_size)
    key_rows, value_rows = in_one_piece((keys_local, values_local), "sp", 0, 1)
    query_pos = seq_index * own_rows + jnp.arange(own_rows, dtype=jnp.int32)
    last_pos = seq_index * own_rows + own_rows - 1
    block_count = (last_pos + span_length - 1) // span_length
    attended = span_attention(
        query_heads,
        query_pos,
        key_rows,
        value_rows,
        head_bias,
        span_segments,
        own_rows,
        block_count,
    ).astype(jnp.bfloat16)
    attended_rows = attended.reshape(own_rows, local_width)
    return sum_at_owner(
        jnp.dot(attended_rows, w_out, preferred_element_type=jnp.float32).astype(jnp.bfloat16),
        "tp",
        0,
    ).astype(jnp.bfloat16)


def solution(mesh):
    placed = (
        P(("sp", "tp"), None),
        P(None, "tp"),
        P(None, "tp"),
        P(None, "tp"),
        P("tp"),
        P("tp", None),
    )
    return jax.shard_map(
        shards, mesh=mesh, in_specs=placed, out_specs=P(("sp", "tp"), None), check_vma=False
    )
```

profile of v0, /device:TPU:240, one launch (start us, length us, event | category | flops | bytes accessed | tf_op | source)
XLA Modules:
  0.0 987.4 jit_solution(5080138480463430278)
XLA Ops:
  7.9 31.3 %all_to_all.10 = bf16[8,64,2048]{2,1,0:T(8,128)(2,1)S(1)} all-to-all(bf16[8,64,2048]{2,1,0:T(8,128)(2,1)S(1)} %broadcast_in_dim.33), channel_id=1, replica_groups=mesh['sp'=32,'tp'=8] {'tp'}, dimensions={0} | all-to-all | bytes 4194304 | tf_op jit(solution)/shard_map/all_to_all | solution.py:9
  41.1 99.9 %all-gather.2.cloned.1.call-done = bf16[16384,256]{0,1:T(8,128)(2,1)} async-done(((bf16[512,256]{0,1:T(8,128)(2,1)}), bf16[16384,256]{0,1:T(8,128)(2,1)}) %all-gather.2.cloned.1.call-update) | async-done | bytes 8388624 | tf_op jit(solution)/shard_map/all_gather | solution.py:26
  141.0 5.8 fusion.34
  146.9 7.8 reshape.78
  154.7 7.8 reshape.76
  162.6 784.6 %while.15 = (s32[]{:T(128)}, f32[512,2,64]{0,2,1:T(8,128)S(1)}, f32[512,2]{0,1:T(2,128)S(1)}, s32[]{:T(128)}, s32[]{:T(128)}, /*index=5*/bf16[16,2,512,2,64]{2,1...) while((s32[]{:T(128)}, f32[512,2,64]{0,2,1:T(8,128)S(1)}, ...), condition=%wide.region_7.8_spmd.clone, body=%wide.region_0.7_spmd.clone.sunk | while | flops 430740992 | bytes 105316672 | solution.py:87
  187.8 6.8 fusion.47
  194.7 25.8 %fusion.48 = f32[512,2,2,4,128]{0,3,2,1,4:T(4,128)S(1)} fusion(f32[512,2,2,4,128]{0,4,3,2,1:T(8,128)} %bitcast.90), kind=kOutput, calls=%fused_computation.18.clone.1 | output fusion | flops 133169152 | bytes 8388608 | tf_op jit(solution)/shard_map/reduce-window.4
  222.6 2.7 broadcast_add_fusion.2
  228.7 4.1 fusion.49
  235.3 6.8 fusion.47
  242.2 25.8 %fusion.48 = f32[512,2,2,4,128]{0,3,2,1,4:T(4,128)S(1)} fusion(f32[512,2,2,4,128]{0,4,3,2,1:T(8,128)} %bitcast.90), kind=kOutput, calls=%fused_computation.18.clone.1 | output fusion | flops 133169152 | bytes 8388608 | tf_op jit(solution)/shard_map/reduce-window.4
  270.0 2.7 broadcast_add_fusion.2
  276.2 4.1 fusion.49
  282.7 6.8 fusion.47
  289.6 25.8 %fusion.48 = f32[512,2,2,4,128]{0,3,2,1,4:T(4,128)S(1)} fusion(f32[512,2,2,4,128]{0,4,3,2,1:T(8,128)} %bitcast.90), kind=kOutput, calls=%fused_computation.18.clone.1 | output fusion | flops 133169152 | bytes 8388608 | tf_op jit(solution)/shard_map/reduce-window.4
  323.7 4.1 fusion.49
  330.2 6.8 fusion.47
  337.1 25.8 %fusion.48 = f32[512,2,2,4,128]{0,3,2,1,4:T(4,128)S(1)} fusion(f32[512,2,2,4,128]{0,4,3,2,1:T(8,128)} %bitcast.90), kind=kOutput, calls=%fused_computation.18.clone.1 | output fusion | flops 133169152 | bytes 8388608 | tf_op jit(solution)/shard_map/reduce-window.4
  364.9 2.7 broadcast_add_fusion.2
  371.1 4.1 fusion.49
  377.6 6.8 fusion.47
  384.6 25.8 %fusion.48 = f32[512,2,2,4,128]{0,3,2,1,4:T(4,128)S(1)} fusion(f32[512,2,2,4,128]{0,4,3,2,1:T(8,128)} %bitcast.90), kind=kOutput, calls=%fused_computation.18.clone.1 | output fusion | flops 133169152 | bytes 8388608 | tf_op jit(solution)/shard_map/reduce-window.4
  412.4 2.7 broadcast_add_fusion.2
  418.6 4.1 fusion.49
  425.1 6.8 fusion.47
  432.0 25.8 %fusion.48 = f32[512,2,2,4,128]{0,3,2,1,4:T(4,128)S(1)} fusion(f32[512,2,2,4,128]{0,4,3,2,1:T(8,128)} %bitcast.90), kind=kOutput, calls=%fused_computation.18.clone.1 | output fusion | flops 133169152 | bytes 8388608 | tf_op jit(solution)/shard_map/reduce-window.4
  466.0 4.1 fusion.49
  472.6 6.8 fusion.47
  479.5 25.8 %fusion.48 = f32[512,2,2,4,128]{0,3,2,1,4:T(4,128)S(1)} fusion(f32[512,2,2,4,128]{0,4,3,2,1:T(8,128)} %bitcast.90), kind=kOutput, calls=%fused_computation.18.clone.1 | output fusion | flops 133169152 | bytes 8388608 | tf_op jit(solution)/shard_map/reduce-window.4
  507.3 2.7 broadcast_add_fusion.2
  513.5 4.1 fusion.49
  520.0 6.8 fusion.47
  526.9 25.8 %fusion.48 = f32[512,2,2,4,128]{0,3,2,1,4:T(4,128)S(1)} fusion(f32[512,2,2,4,128]{0,4,3,2,1:T(8,128)} %bitcast.90), kind=kOutput, calls=%fused_computation.18.clone.1 | output fusion | flops 133169152 | bytes 8388608 | tf_op jit(solution)/shard_map/reduce-window.4
  554.8 2.7 broadcast_add_fusion.2
  561.0 4.1 fusion.49
  567.5 6.8 fusion.47
  574.4 25.8 %fusion.48 = f32[512,2,2,4,128]{0,3,2,1,4:T(4,128)S(1)} fusion(f32[512,2,2,4,128]{0,4,3,2,1:T(8,128)} %bitcast.90), kind=kOutput, calls=%fused_computation.18.clone.1 | output fusion | flops 133169152 | bytes 8388608 | tf_op jit(solution)/shard_map/reduce-window.4
  608.4 4.1 fusion.49
  614.9 6.8 fusion.47
  621.9 25.8 %fusion.48 = f32[512,2,2,4,128]{0,3,2,1,4:T(4,128)S(1)} fusion(f32[512,2,2,4,128]{0,4,3,2,1:T(8,128)} %bitcast.90), kind=kOutput, calls=%fused_computation.18.clone.1 | output fusion | flops 133169152 | bytes 8388608 | tf_op jit(solution)/shard_map/reduce-window.4
  649.7 2.7 broadcast_add_fusion.2
  655.9 4.1 fusion.49
  662.4 6.8 fusion.47
  669.3 25.8 %fusion.48 = f32[512,2,2,4,128]{0,3,2,1,4:T(4,128)S(1)} fusion(f32[512,2,2,4,128]{0,4,3,2,1:T(8,128)} %bitcast.90), kind=kOutput, calls=%fused_computation.18.clone.1 | output fusion | flops 133169152 | bytes 8388608 | tf_op jit(solution)/shard_map/reduce-window.4
  703.4 4.1 fusion.49
  709.9 6.8 fusion.47
  716.8 25.8 %fusion.48 = f32[512,2,2,4,128]{0,3,2,1,4:T(4,128)S(1)} fusion(f32[512,2,2,4,128]{0,4,3,2,1:T(8,128)} %bitcast.90), kind=kOutput, calls=%fused_computation.18.clone.1 | output fusion | flops 133169152 | bytes 8388608 | tf_op jit(solution)/shard_map/reduce-window.4
  744.6 2.7 broadcast_add_fusion.2
  750.8 4.1 fusion.49
  757.3 6.8 fusion.47
  764.2 25.8 %fusion.48 = f32[512,2,2,4,128]{0,3,2,1,4:T(4,128)S(1)} fusion(f32[512,2,2,4,128]{0,4,3,2,1:T(8,128)} %bitcast.90), kind=kOutput, calls=%fused_computation.18.clone.1 | output fusion | flops 133169152 | bytes 8388608 | tf_op jit(solution)/shard_map/reduce-window.4
  792.1 2.7 broadcast_add_fusion.2
  798.3 4.1 fusion.49
  804.8 6.8 fusion.47
  811.7 25.8 %fusion.48 = f32[512,2,2,4,128]{0,3,2,1,4:T(4,128)S(1)} fusion(f32[512,2,2,4,128]{0,4,3,2,1:T(8,128)} %bitcast.90), kind=kOutput, calls=%fused_computation.18.clone.1 | output fusion | flops 133169152 | bytes 8388608 | tf_op jit(solution)/shard_map/reduce-window.4
  845.7 4.1 fusion.49
  852.2 6.8 fusion.47
  859.2 25.8 %fusion.48 = f32[512,2,2,4,128]{0,3,2,1,4:T(4,128)S(1)} fusion(f32[512,2,2,4,128]{0,4,3,2,1:T(8,128)} %bitcast.90), kind=kOutput, calls=%fused_computation.18.clone.1 | output fusion | flops 133169152 | bytes 8388608 | tf_op jit(solution)/shard_map/reduce-window.4
  893.2 4.1 fusion.49
  899.7 6.8 fusion.47
  906.6 25.8 %fusion.48 = f32[512,2,2,4,128]{0,3,2,1,4:T(4,128)S(1)} fusion(f32[512,2,2,4,128]{0,4,3,2,1:T(8,128)} %bitcast.90), kind=kOutput, calls=%fused_computation.18.clone.1 | output fusion | flops 133169152 | bytes 8388608 | tf_op jit(solution)/shard_map/reduce-window.4
  940.7 4.1 fusion.49
  948.0 31.3 %all_to_all.11 = bf16[8,64,2048]{2,1,0:T(8,128)(2,1)S(1)} all-to-all(bf16[8,64,2048]{2,1,0:T(8,128)(2,1)S(1)} %bitcast.92), channel_id=1, replica_groups=mesh['sp'=32,'tp'=8] {'tp'}, dimensions={0} | all-to-all | bytes 4194304 | tf_op jit(solution)/shard_map/all_to_all | solution.py:37
  (335 shorter events, 149.2 us)
Async XLA Ops:
  6.5 940.7 %copy-start = (bf16[128,2048]{1,0:T(8,128)(2,1)S(1)}, bf16[128,2048]{1,0:T(8,128)(2,1)}, u32[]{:S(2)}) copy-start(bf16[128,2048]{1,0:T(8,128)(2,1)} %param.13) | copy-start | bytes 1572868
  6.5 32.7 %copy-start.6 = (bf16[2048,128]{1,0:T(8,128)(2,1)S(1)}, bf16[2048,128]{1,0:T(8,128)(2,1)}, u32[]{:S(2)}) copy-start(bf16[2048,128]{1,0:T(8,128)(2,1)} %param.11) | copy-start | bytes 1572868
  6.5 32.7 %copy-start.7 = (bf16[2048,128]{1,0:T(8,128)(2,1)S(1)}, bf16[2048,128]{1,0:T(8,128)(2,1)}, u32[]{:S(2)}) copy-start(bf16[2048,128]{1,0:T(8,128)(2,1)} %param.10) | copy-start | bytes 1572868
  6.5 32.7 %copy-start.8 = (bf16[2048,128]{1,0:T(8,128)(2,1)S(1)}, bf16[2048,128]{1,0:T(8,128)(2,1)}, u32[]{:S(2)}) copy-start(bf16[2048,128]{1,0:T(8,128)(2,1)} %param.9) | copy-start | bytes 1572868
  6.5 134.5 %all-gather.2.cloned.1.call-start = ((), (), s32[]{:S(2)}) async-start(), calls=%async_computation.2 | async-start | bytes 8650752 | tf_op jit(solution)/shard_map/all_gather | solution.py:26
  40.3 106.6 %copy-start.4 = (bf16[512,384]{0,1:T(8,128)(2,1)}, bf16[512,384]{0,1:T(8,128)(2,1)S(1)}, u32[]{:S(2)}) copy-start(bf16[512,384]{0,1:T(8,128)(2,1)S(1)} %fusion.28) | copy-start | bytes 1179652
  154.7 7.9 slice-start
  154.7 7.9 copy-start.5
  220.5 1.9 copy-start.1
  225.3 2.5 copy-start.2
  225.3 3.5 copy-start.3
  268.0 1.9 copy-start.1
  272.7 2.5 copy-start.2
  272.7 3.5 copy-start.3
  315.5 1.9 copy-start.1
  320.2 2.5 copy-start.2
  320.2 3.5 copy-start.3
  362.9 1.9 copy-start.1
  367.7 2.5 copy-start.2
  367.7 3.5 copy-start.3
  410.4 1.9 copy-start.1
  415.1 2.5 copy-start.2
  415.1 3.5 copy-start.3
  457.9 1.9 copy-start.1
  462.6 2.5 copy-start.2
  462.6 3.5 copy-start.3
  505.3 1.9 copy-start.1
  510.0 2.5 copy-start.2
  510.1 3.5 copy-start.3
  552.8 1.9 copy-start.1
  557.5 2.5 copy-start.2
  557.5 3.5 copy-start.3
  600.2 1.9 copy-start.1
  605.0 2.5 copy-start.2
  605.0 3.5 copy-start.3
  647.7 1.9 copy-start.1
  652.4 2.5 copy-start.2
  652.4 3.5 copy-start.3
  695.2 1.9 copy-start.1
  699.9 2.5 copy-start.2
  699.9 3.5 copy-start.3
  742.6 1.9 copy-start.1
  747.3 2.5 copy-start.2
  747.4 3.5 copy-start.3
  790.1 1.9 copy-start.1
  794.8 2.5 copy-start.2
  794.8 3.5 copy-start.3
  837.5 1.9 copy-start.1
  842.3 2.5 copy-start.2
  842.3 3.5 copy-start.3
  885.0 1.9 copy-start.1
  889.7 2.5 copy-start.2
  889.7 3.5 copy-start.3
  932.5 1.9 copy-start.1
  937.2 2.5 copy-start.2
  937.2 3.5 copy-start.3
Sparse Core Ops, SparseCore 0:
  41.2 99.7 all-gather.1
where the time goes:
time: 992 us; the launch traced here: 987 us
  other arithmetic  533 us (54%)
  local copies, waits for them, and re-layouts  132 us (13%)
  matrix products  119 us (12%)
  waiting for transfers between devices  100 us (10%)
  blocking collectives  62.6 us (6%)
  loops' own time  27.5 us (3%)
  between operations  13.7 us (1%)
    another operation x32, other arithmetic  414 us
    dot_general x16, matrix products, segment_terms(): jnp.einsum('rhd,sthd->rhst', query_rows, key_span, preferred_element_type...  109 us
    all_gather x1, waiting for transfers between devices, in_one_piece(): out = lax.all_gather(both, axis, axis=dim, tiled=True)  99.9 us
    convert_element_type x16, other arithmetic, segment_terms(): jnp.where(causal, jnp.exp(jax.nn.log_sigmoid(scores) + tail), 0.0)  65.9 us
    while x96, local copies, waits for them, and re-layouts  46.8 us
    another operation x16, other arithmetic, segment_terms(): tail = lax.cumsum(log_keep, axis=3, reverse=True) - log_keep  43.2 us
    another operation x16, local copies, waits for them, and re-layouts, segment_terms(): tail = lax.cumsum(log_keep, axis=3, reverse=True) - log_keep  38.9 us
    all_to_all x1, blocking collectives, copy_for_each(): return lax.all_to_all(copies, axis, split_axis=0, concat_axis=0, tiled=True)  31.3 us
  transfers between devices with their start and end apart: 1, of which 1 were waited for; matrix products, arithmetic and copies ran while one was open for 0% of the time, Pallas kernels for 0%

commit v1 on v0

v1 whole, which is shorter than its diff:
```python
import jax, jax.numpy as jnp
from jax import lax
from jax.sharding import PartitionSpec as P
from jax.experimental import pallas as pl
from jax.experimental.pallas import tpu as pltpu

LOG2E = 1.4426950408889634
SEG = 512
N_UNITS = 34
NEG = -1e30

def build_tables(bias2, c, mask_ref, tri_ref):
    rows = lax.broadcasted_iota(jnp.int32, (256, SEG), 0)
    cols = lax.broadcasted_iota(jnp.int32, (256, SEG), 1)
    qpos = (2 * (rows // 64) + c) * 64 + rows % 64
    mask_ref[0] = jnp.full((256, SEG), bias2, jnp.float32)
    mask_ref[1] = jnp.where(cols < qpos, bias2, NEG)
    mask_ref[2] = jnp.full((256, SEG), NEG, jnp.float32)
    j = lax.broadcasted_iota(jnp.int32, (SEG, SEG), 0)
    s = lax.broadcasted_iota(jnp.int32, (SEG, SEG), 1)
    tri_ref[...] = jnp.where(j > s, -1.0, 0.0).astype(jnp.bfloat16)

def attend(z, q_ref, kv_ref, mask_ref, tri_ref, sp_ref, ls_ref, w_ref, f_ref, acc_ref, RC=128):
    n_a = 4 * z + 2
    zm = 7 - z

    def place(n):
        is_b = (n >= n_a).astype(jnp.int32)
        s = n - is_b * n_a
        first = is_b * (4 * zm + 2) + (1 - is_b) * (4 * z)
        return is_b, s, first

    def stage1(n):
        is_b, s, first = place(n)
        slot = n % 2
        kv = kv_ref[s]
        for r in range(0, 512, RC):
            half = r // 256
            b = first + half
            idx = (s >= b).astype(jnp.int32) + (s > b).astype(jnp.int32)
            q = q_ref[pl.ds(pl.multiple_of(is_b * 512, 512) + r, RC), :]
            sc = lax.dot_general(q, kv, (((1,), (1,)), ((), ())), preferred_element_type=jnp.float32)
            sc = sc + mask_ref[idx, pl.ds(r % 256, RC), :]
            l = jnp.log2(1.0 + jnp.exp2(jnp.minimum(sc, 126.0)))
            sp = jnp.maximum(l, sc)
            sp_ref[slot, pl.ds(r, RC), :] = sp.astype(jnp.bfloat16)
            ls_ref[slot, pl.ds(r, RC), :] = sc - sp

    def stage2(n):
        slot = n % 2
        for r in range(0, 512, RC):
            sp = sp_ref[slot, pl.ds(r, RC), :]
            lo = jnp.dot(sp, tri_ref[:, 0:256], preferred_element_type=jnp.float32)
            hi = jnp.dot(sp[:, 256:], tri_ref[256:, 256:], preferred_element_type=jnp.float32)
            w_ref[slot, pl.ds(r, RC), 0:256] = jnp.exp2(ls_ref[slot, pl.ds(r, RC), 0:256] + lo).astype(jnp.bfloat16)
            w_ref[slot, pl.ds(r, RC), 256:512] = jnp.exp2(ls_ref[slot, pl.ds(r, RC), 256:512] + hi).astype(jnp.bfloat16)
            keep = lo[:, 0:1] - sp[:, 0:1].astype(jnp.float32)
            f_ref[slot, pl.ds(r, RC), :] = jnp.exp2(jnp.broadcast_to(keep, (RC, 128)))

    def stage3(n):
        is_b, s, _ = place(n)
        slot = n % 2
        kv = kv_ref[s]
        for r in range(0, 512, RC):
            rows = pl.ds(pl.multiple_of(is_b * 512, 512) + r, RC)
            pv = jnp.dot(w_ref[slot, pl.ds(r, RC), :], kv, preferred_element_type=jnp.float32)
            acc_ref[rows, :] = acc_ref[rows, :] * f_ref[slot, pl.ds(r, RC), :] + pv

    acc_ref[...] = jnp.zeros_like(acc_ref)
    stage1(0)
    stage2(0)
    stage1(1)

    def body(i, carry):
        stage3(i)
        stage2(i + 1)
        stage1(i + 2)
        return carry

    lax.fori_loop(0, N_UNITS - 2, body, 0)
    stage3(N_UNITS - 2)
    stage2(N_UNITS - 1)
    stage3(N_UNITS - 1)

SCRATCH = lambda: [
    pltpu.VMEM((3, 256, SEG), jnp.float32),
    pltpu.VMEM((SEG, SEG), jnp.bfloat16),
    pltpu.VMEM((2, 512, SEG), jnp.bfloat16),
    pltpu.VMEM((2, 512, SEG), jnp.float32),
    pltpu.VMEM((2, 512, SEG), jnp.bfloat16),
    pltpu.VMEM((2, 512, 128), jnp.float32),
    pltpu.VMEM((1024, 128), jnp.float32),
]


def kernel(b_ref, q_ref, kv_ref, o_ref, mask_ref, tri_ref, sp_ref, ls_ref, w_ref, f_ref, acc_ref):
    z = lax.axis_index("sp") // 4
    c = lax.axis_index("tp") % 2
    build_tables(b_ref[0] * LOG2E, c, mask_ref, tri_ref)
    attend(z, q_ref, kv_ref, mask_ref, tri_ref, sp_ref, ls_ref, w_ref, f_ref, acc_ref)
    o_ref[...] = acc_ref[...].astype(jnp.bfloat16)


def shards(tokens, w_query, w_key, w_value, head_bias, w_out):
    same_core = [[0, 2, 4, 6], [1, 3, 5, 7]]
    pair = [[0, 1], [2, 3], [4, 5], [6, 7]]
    along_y = [[4 * z + y for y in range(4)] for z in range(8)]
    along_z = [[4 * z + y for z in range(8)] for y in range(4)]
    mirror = [(4 * z + y, 4 * (7 - z) + y) for z in range(8) for y in range(4)]
    y = lax.axis_index("sp") % 4
    rows = lax.all_gather(tokens, "tp", axis_index_groups=same_core, axis=0, tiled=True)
    own = jnp.concatenate([w_query.reshape(-1, 2, 64), w_key.reshape(-1, 2, 64), w_value.reshape(-1, 2, 64)], axis=2)
    both = lax.all_gather(own, "tp", axis_index_groups=pair, axis=1, tiled=True)
    bias = lax.all_gather(head_bias, "tp", axis_index_groups=pair, axis=0, tiled=True)
    full_out = lax.all_gather(w_out, "tp", axis=0, tiled=True)
    qkv = jnp.dot(rows, both.reshape(-1, 768), preferred_element_type=jnp.float32).reshape(256, 4, 192)
    scale = jnp.where(jnp.arange(192) < 64, LOG2E / 8, 1.0)
    qkv = jnp.moveaxis((qkv * scale).astype(jnp.bfloat16), 1, 0)
    qkv = lax.all_to_all(qkv, "sp", 0, 0, axis_index_groups=along_y, tiled=True)
    q, kv = qkv[..., :64], qkv[..., 64:]
    away = lax.ppermute(q[2:], "sp", mirror)
    q = jnp.concatenate([q[:2], away], axis=0).reshape(1024, 64)
    q = jnp.pad(q, ((0, 0), (0, 64)))
    kv = lax.all_gather(kv, "sp", axis_index_groups=along_z, axis=0, tiled=True)
    kv = lax.all_gather(kv.reshape(32, 4, 64, 128), "tp", axis_index_groups=pair, axis=0)
    kv = jnp.moveaxis(kv, 0, 2).reshape(32, 512, 128)
    out = pl.pallas_call(
        kernel,
        out_shape=jax.ShapeDtypeStruct((1024, 128), jnp.bfloat16),
        in_specs=[pl.BlockSpec(memory_space=pltpu.SMEM)] + [pl.BlockSpec(memory_space=pltpu.VMEM)] * 2,
        out_specs=pl.BlockSpec(memory_space=pltpu.VMEM),
        scratch_shapes=SCRATCH(),
        compiler_params=pltpu.CompilerParams(vmem_limit_bytes=48 * 2**20),
        cost_estimate=pl.CostEstimate(flops=40 * 10**9, bytes_accessed=5 * 10**6, transcendentals=0),
        name="attn",
    )(lax.dynamic_slice_in_dim(bias, y, 1), q, kv)
    out = out[:, 64:].reshape(4, 4, 64, 64)
    out = jnp.concatenate([out[:2], lax.ppermute(out[2:], "sp", mirror)], axis=0)
    out = lax.all_to_all(out, "sp", 0, 0, axis_index_groups=along_y, tiled=True)
    out = lax.all_to_all(out, "tp", 1, 1, axis_index_groups=same_core, tiled=True)
    out = jnp.transpose(out, (2, 1, 0, 3)).reshape(64, 1024)
    return jnp.dot(out, full_out, preferred_element_type=jnp.float32).astype(jnp.bfloat16)


def solution(mesh):
    placed = (P(("sp", "tp"), None), P(None, "tp"), P(None, "tp"), P(None, "tp"), P("tp"), P("tp", None))
    return jax.shard_map(
        shards, mesh=mesh, in_specs=placed, out_specs=P(("sp", "tp"), None), check_vma=False
    )
```

time: 992 us -> 207 us (0.21)
  the two profiles are of different devices: /device:TPU:240 before, /device:TPU:2 now
where the time goes in v1:
time: 207 us
  waiting for transfers between devices  106 us (51%)
  blocking collectives  34.2 us (17%)
  Pallas kernels  28 us (14%)
  between operations  14 us (7%)
  local copies, waits for them, and re-layouts  10.3 us (5%)
  matrix products  6.92 us (3%)
  starting transfers between devices  5.71 us (3%)
    all_gather x1, waiting for transfers between devices, shards(): kv = lax.all_gather(kv, 'sp', axis_index_groups=along_z, axis=0, tiled=True)  40.4 us
    pallas_call x1, Pallas kernels, shards(): pl.pallas_call(kernel, out_shape=jax.ShapeDtypeStruct((1024, 128), jnp.bf...  28 us
    all_gather x1, waiting for transfers between devices, shards(): lax.all_gather(tokens, 'tp', axis_index_groups=same_core, axis=0, tiled=T...  25.2 us
    all_gather x1, waiting for transfers between devices, shards(): both = lax.all_gather(own, 'tp', axis_index_groups=pair, axis=1, tiled=True)  20.8 us
    all_to_all x1, blocking collectives, shards(): qkv = lax.all_to_all(qkv, 'sp', 0, 0, axis_index_groups=along_y, tiled=True)  12.6 us
    all_gather x1, waiting for transfers between devices, shards(): lax.all_gather(kv.reshape(32, 4, 64, 128), 'tp', axis_index_groups=pair,...  11.7 us
    all_to_all x1, blocking collectives, shards(): out = lax.all_to_all(out, 'sp', 0, 0, axis_index_groups=along_y, tiled=True)  10.1 us
    all_to_all x1, blocking collectives, shards(): lax.all_to_all(out, 'tp', 1, 1, axis_index_groups=same_core, tiled=True)  9.12 us
  transfers between devices with their start and end apart: 7, of which 5 were waited for; matrix products, arithmetic and copies ran while one was open for 4% of the time, Pallas kernels for 14%

profile of v1, /device:TPU:2, one launch (start us, length us, event | category | flops | bytes accessed | tf_op | source)
XLA Modules:
  0.0 206.8 jit_solution(18001401403015637148)
XLA Ops:
  6.5 0.0 all-gather.8.cloned.1.call-start
  6.5 0.7 all-gather.8.cloned.1.call-update
  7.3 0.0 all-gather.6.cloned.1.call-start
  7.3 1.2 copy.14
  8.6 1.2 copy.15
  9.8 1.2 copy.16
  11.1 1.3 pad_maximum_fusion
  12.3 0.0 all-gather.6.cloned.1.call-update
  12.3 0.0 all-gather.10.cloned.1.call-start
  12.4 25.2 %all-gather.8.cloned.1.call-done = bf16[256,2048]{1,0:T(8,128)(2,1)} async-done(((bf16[64,2048]{1,0:T(8,128)(2,1)}), bf16[256,2048]{1,0:T(8,128)(2,1)}) %all-gather.8.cloned.1.call-update) | async-done | bytes 1048592 | tf_op jit(solution)/shard_map/all_gather | solution.py:111
  37.6 20.8 %all-gather.6.cloned.1.call-done = bf16[2048,4,192]{0,2,1:T(8,128)(2,1)} async-done(((bf16[2048,2,192]{0,2,1:T(8,128)(2,1)}), bf16[2048,4,192]{0,2,1:T(8,128)(2,1)}) %all-gather.6.cloned.1.call-update) | async-done | bytes 3145744 | tf_op jit(solution)/shard_map/all_gather | solution.py:113
  58.4 3.2 %fusion.4 = f32[768,256]{1,0:T(8,128)S(1)} fusion(bf16[2048,768]{0,1:T(8,128)(2,1)} %bitcast.44, bf16[256,2048]{1,0:T(8,128)(2,1)} %all-gather.8.cloned.1.call-done), kind=kOutput, calls=%fused_computation.12 | convolution fusion | flops 805306368 | bytes 4980736 | tf_op jit(solution)/shard_map/dot_general | solution.py:116
  61.6 0.0 copy-start.2
  61.6 0.0 copy-start.1
  61.6 0.1 fusion
  61.8 12.6 %all_to_all.15 = bf16[4,256,192]{1,2,0:T(8,128)(2,1)S(1)} all-to-all(bf16[4,256,192]{1,2,0:T(8,128)(2,1)S(1)} %fusion), channel_id=1, replica_groups={{0,8,16,24},{32,40,48,56},{64,72,80,88},{96,104,112,120},{128,136,144,1..., dimensions={0} | all-to-all | bytes 786432 | tf_op jit(solution)/shard_map/all_to_all | solution.py:119
  74.4 0.8 copy.18
  75.2 0.0 all-gather.10.cloned.1.call-update
  75.3 0.0 all-gather.12.cloned.1.call-start
  75.3 40.4 %all-gather.10.cloned.1.call-done = bf16[32,256,128]{2,1,0:T(8,128)(2,1)} async-done(((bf16[4,256,128]{2,1,0:T(8,128)(2,1)}), bf16[32,256,128]{2,1,0:T(8,128)(2,1)}) %all-gather.10.cloned.1.call-update) | async-done | bytes 2097168 | tf_op jit(solution)/shard_map/all_gather | solution.py:124
  115.7 0.0 all-gather.12.cloned.1.call-update
  115.7 0.0 all-gather.14.cloned.1.call-start
  115.8 0.5 all-gather.14.cloned.1.call-update
  116.3 2.2 %collective-permute-start = (bf16[2,256,64]{1,2,0:T(8,128)(2,1)S(1)}, bf16[2,256,64]{1,2,0:T(8,128)(2,1)S(1)}, u32[]{:S(2)}, u32[]{:S(2)}) collective-permute-start(bf16[2,256,64]{1,2,0:T(8,128)(2,1)S(1)} %get-tuple-element.6), channel_id=1, source_target_pairs={{0,224},{8,232},{16,240},{24,248},{32,192},{40,200},{48,208},{56,2... | collective-permute-start | bytes 196616 | tf_op jit(solution)/shard_map/ppermute | solution.py:121
  118.5 0.0 copy-done.2
  118.5 0.6 dynamic-slice
  119.7 0.0 copy-done.1
  119.8 0.2 dynamic-update-slice
  120.0 2.4 %all-reduce.1 = f32[4]{0:T(128)S(1)} all-reduce(f32[4]{0:T(128)S(1)} %dynamic-update-slice), channel_id=1, replica_groups={{0,1},{2,3},{4,5},{6,7},{8,9},{10,11},{12,13},{14,15},{16,17},{18,19},{..., use_global_device_ids=true, to_apply=%add.1 | all-reduce | flops 4 | bytes 32
  122.4 0.6 dynamic_slice.3.b_ref
  123.0 0.0 collective-permute-done
  123.1 0.2 copy.17
  123.2 0.1 pad.4.q_ref
  123.3 11.7 %all-gather.12.cloned.1.call-done = bf16[2,32,4,64,128]{4,3,0,2,1:T(8,128)(2,1)} async-done(((bf16[1,32,4,64,128]{4,3,0,2,1:T(8,128)(2,1)}), bf16[2,32,4,64,128]{4,3,0,2,1:T(8,128)(2,1)}) %all-gather.12.cloned.1.call-update) | async-done | bytes 4194320 | tf_op jit(solution)/shard_map/all_gather | solution.py:125
  135.0 0.0 copy-start
  135.0 2.2 %copy-done = bf16[2,32,4,64,128]{4,3,0,2,1:T(8,128)(2,1)S(1)} copy-done((bf16[2,32,4,64,128]{4,3,0,2,1:T(8,128)(2,1)S(1)}, bf16[2,32,4,64,128]{4,3,0,2,1:T(8,128)(2,1)}, u32[]{:S(2)}) %copy-start) | copy-done | bytes 4194328
  137.2 28.0 %attn.1 = bf16[1024,128]{1,0:T(8,128)(2,1)S(1)} custom-call(f32[1]{0:T(128)} %dynamic_slice.3.b_ref, bf16[1024,128]{1,0:T(8,128)(2,1)S(1)} %pad.4.q_ref, bf16[32,512,128]{2,1,0:T(8,128)(2,1)S(1)} %bitcast.33), custom_call_target="tpu_custom_call" | custom-call | flops 40000000000 | bytes 5000000 | tf_op jit(solution)/shard_map/attn/pallas_call | solution.py:127
  165.2 0.1 fusion.2
  165.3 0.1 copy.20
  165.5 3.4 %collective-permute-start.1 = (bf16[2,4,64,64]{3,1,2,0:T(4,128)(2,1)S(1)}, bf16[2,4,64,64]{3,1,2,0:T(4,128)(2,1)S(1)}, u32[]{:S(2)}, u32[]{:S(2)}) collective-permute-start(bf16[2,4,64,64]{3,1,2,0:T(4,128)(2,1)S(1)} %copy.20), channel_id=1, source_target_pairs={{0,224},{8,232},{16,240},{24,248},{32,192},{40,200},{48,208},{56,2... | collective-permute-start | bytes 196616 | tf_op jit(solution)/shard_map/ppermute | solution.py:138
  168.9 0.1 copy.21
  169.0 6.7 %collective-permute-done.1 = bf16[2,4,64,64]{3,1,2,0:T(4,128)(2,1)S(1)} collective-permute-done((bf16[2,4,64,64]{3,1,2,0:T(4,128)(2,1)S(1)}, bf16[2,4,64,64]{3,1,2,0:T(4,128)(2,1)S(1)}, u32[]{:S(2)}, u32[]{:S(2)}) %collective-permute-start.1) | collective-permute-done | bytes 65568 | tf_op jit(solution)/shard_map/ppermute | solution.py:138
  175.6 0.2 fusion.3
  175.8 0.2 reshape.45
  176.1 10.1 %all_to_all.16 = bf16[4,2,8192]{2,1,0:T(2,128)(2,1)S(1)} all-to-all(bf16[4,2,8192]{2,1,0:T(2,128)(2,1)S(1)} %reshape.45), channel_id=1, replica_groups={{0,8,16,24},{32,40,48,56},{64,72,80,88},{96,104,112,120},{128,136,144,1..., dimensions={0} | all-to-all | bytes 262144 | tf_op jit(solution)/shard_map/all_to_all | solution.py:139
  186.1 0.2 reshape.46
  186.3 0.2 copy.25
  186.6 0.2 reshape.47
  186.8 9.1 %all_to_all.17 = bf16[4,2,8192]{2,1,0:T(2,128)(2,1)S(1)} all-to-all(bf16[4,2,8192]{2,1,0:T(2,128)(2,1)S(1)} %reshape.47), channel_id=1, replica_groups={{0,2,4,6},{1,3,5,7},{8,10,12,14},{9,11,13,15},{16,18,20,22},{17,19,21,2..., dimensions={0} | all-to-all | bytes 262144 | tf_op jit(solution)/shard_map/all_to_all | solution.py:140
  195.9 0.2 reshape.48
  196.1 0.1 bitcast_bitcast_fusion
  196.2 0.1 copy.23
  196.3 0.2 reshape.39
  196.5 0.0 all-gather.14.cloned.1.call-done
  196.6 3.7 %convolution_convert_fusion = bf16[64,2048]{1,0:T(8,128)(2,1)} fusion(bf16[64,1024]{1,0:T(8,128)(2,1)S(1)} %reshape.39, bf16[1024,2048]{1,0:T(8,128)(2,1)} %all-gather.14.cloned.1.call-done), kind=kOutput, calls=%fused_computation | convolution fusion | flops 268566528 | bytes 4587520 | tf_op jit(solution)/shard_map/dot_general | solution.py:142
  (5 shorter events, 0.0 us)
Async XLA Ops:
  6.5 31.1 %all-gather.8.cloned.1.call-start = ((), (), s32[]{:S(2)}) async-start(), calls=%async_computation.4 | async-start | bytes 1310720 | tf_op jit(solution)/shard_map/all_gather | solution.py:111
  7.3 51.2 %all-gather.6.cloned.1.call-start = ((), (), s32[]{:S(2)}) async-start(), calls=%async_computation.3 | async-start | bytes 4718592 | tf_op jit(solution)/shard_map/all_gather | solution.py:113
  12.3 103.4 %all-gather.10.cloned.1.call-start = ((), (), s32[]{:S(2)}) async-start(), calls=%async_computation.5 | async-start | bytes 2359296 | tf_op jit(solution)/shard_map/all_gather | solution.py:124
  61.6 56.9 %copy-start.2 = (u32[256]{0:T(256)S(1)}, u32[256]{0:T(256)}, u32[]{:S(2)}) copy-start(u32[256]{0:T(256)} %constant.34) | copy-start | bytes 3076
  61.6 58.1 %copy-start.1 = (f32[2]{0:T(128)S(1)}, f32[2]{0:T(128)}, u32[]{:S(2)}) copy-start(f32[2]{0:T(128)} %param.10) | copy-start | bytes 28
  75.3 59.7 %all-gather.12.cloned.1.call-start = ((), (), s32[]{:S(2)}) async-start(), calls=%async_computation.6 | async-start | bytes 6291456 | tf_op jit(solution)/shard_map/all_gather | solution.py:125
  115.7 80.8 %all-gather.14.cloned.1.call-start = ((), (), s32[]{:S(2)}) async-start(), calls=%async_computation.7 | async-start | bytes 4718592 | tf_op jit(solution)/shard_map/all_gather | solution.py:115
  116.3 6.7 %collective-permute-start = (bf16[2,256,64]{1,2,0:T(8,128)(2,1)S(1)}, bf16[2,256,64]{1,2,0:T(8,128)(2,1)S(1)}, u32[]{:S(2)}, u32[]{:S(2)}) collective-permute-start(bf16[2,256,64]{1,2,0:T(8,128)(2,1)S(1)} %get-tuple-element.6), channel_id=1, source_target_pairs={{0,224},{8,232},{16,240},{24,248},{32,192},{40,200},{48,208},{56,2... | collective-permute-start | bytes 196616 | tf_op jit(solution)/shard_map/ppermute | solution.py:121
  135.0 2.2 %copy-start = (bf16[2,32,4,64,128]{4,3,0,2,1:T(8,128)(2,1)S(1)}, bf16[2,32,4,64,128]{4,3,0,2,1:T(8,128)(2,1)}, u32[]{:S(2)}) copy-start(bf16[2,32,4,64,128]{4,3,0,2,1:T(8,128)(2,1)} %all-gather.12.cloned.1.call-done) | copy-start | bytes 12582916
  165.5 10.2 %collective-permute-start.1 = (bf16[2,4,64,64]{3,1,2,0:T(4,128)(2,1)S(1)}, bf16[2,4,64,64]{3,1,2,0:T(4,128)(2,1)S(1)}, u32[]{:S(2)}, u32[]{:S(2)}) collective-permute-start(bf16[2,4,64,64]{3,1,2,0:T(4,128)(2,1)S(1)} %copy.20), channel_id=1, source_target_pairs={{0,224},{8,232},{16,240},{24,248},{32,192},{40,200},{48,208},{56,2... | collective-permute-start | bytes 196616 | tf_op jit(solution)/shard_map/ppermute | solution.py:138
Sparse Core Ops, SparseCore 0:
  9.1 28.4 all-gather.7
  39.4 18.9 all-gather.5
  75.4 40.2 all-gather.9
  117.4 17.5 all-gather.11
  136.7 34.8 all-gather.13

commit v2 on v1

v2 whole, which is shorter than its diff:
```python
import jax, jax.numpy as jnp
from jax import lax
from jax.sharding import PartitionSpec as P
from jax.experimental import pallas as pl
from jax.experimental.pallas import tpu as pltpu

LOG2E = 1.4426950408889634
SEG = 512
N_UNITS = 34
NEG = -1e30

def build_tables(bias2, c, mask_ref, tri_ref):
    rows = lax.broadcasted_iota(jnp.int32, (256, SEG), 0)
    cols = lax.broadcasted_iota(jnp.int32, (256, SEG), 1)
    qpos = (2 * (rows // 64) + c) * 64 + rows % 64
    mask_ref[0] = jnp.full((256, SEG), bias2, jnp.float32)
    mask_ref[1] = jnp.where(cols < qpos, bias2, NEG)
    mask_ref[2] = jnp.full((256, SEG), NEG, jnp.float32)
    j = lax.broadcasted_iota(jnp.int32, (SEG, SEG), 0)
    s = lax.broadcasted_iota(jnp.int32, (SEG, SEG), 1)
    tri_ref[...] = jnp.where(j > s, -1.0, 0.0).astype(jnp.bfloat16)

def attend(z, q_ref, kv_ref, mask_ref, tri_ref, sp_ref, ls_ref, w_ref, f_ref, acc_ref, RC=128):
    n_a = 4 * z + 2
    zm = 7 - z

    def place(n):
        is_b = (n >= n_a).astype(jnp.int32)
        s = n - is_b * n_a
        first = is_b * (4 * zm + 2) + (1 - is_b) * (4 * z)
        return is_b, s, first

    def stage1(n):
        is_b, s, first = place(n)
        slot = n % 2
        kv = kv_ref[s].reshape(SEG, 128)
        for r in range(0, 512, RC):
            half = r // 256
            b = first + half
            idx = (s >= b).astype(jnp.int32) + (s > b).astype(jnp.int32)
            q = q_ref[pl.ds(pl.multiple_of(is_b * 512, 512) + r, RC), :]
            sc = lax.dot_general(q, kv, (((1,), (1,)), ((), ())), preferred_element_type=jnp.float32)
            sc = sc + mask_ref[idx, pl.ds(r % 256, RC), :]
            l = jnp.log2(1.0 + jnp.exp2(jnp.minimum(sc, 126.0)))
            sp = jnp.maximum(l, sc)
            sp_ref[slot, pl.ds(r, RC), :] = sp.astype(jnp.bfloat16)
            ls_ref[slot, pl.ds(r, RC), :] = sc - sp

    def stage2(n):
        slot = n % 2
        for r in range(0, 512, RC):
            sp = sp_ref[slot, pl.ds(r, RC), :]
            lo = jnp.dot(sp, tri_ref[:, 0:256], preferred_element_type=jnp.float32)
            hi = jnp.dot(sp[:, 256:], tri_ref[256:, 256:], preferred_element_type=jnp.float32)
            w_ref[slot, pl.ds(r, RC), 0:256] = jnp.exp2(ls_ref[slot, pl.ds(r, RC), 0:256] + lo).astype(jnp.bfloat16)
            w_ref[slot, pl.ds(r, RC), 256:512] = jnp.exp2(ls_ref[slot, pl.ds(r, RC), 256:512] + hi).astype(jnp.bfloat16)
            keep = lo[:, 0:1] - sp[:, 0:1].astype(jnp.float32)
            f_ref[slot, pl.ds(r, RC), :] = jnp.exp2(jnp.broadcast_to(keep, (RC, 128)))

    def stage3(n):
        is_b, s, _ = place(n)
        slot = n % 2
        kv = kv_ref[s].reshape(SEG, 128)
        for r in range(0, 512, RC):
            rows = pl.ds(pl.multiple_of(is_b * 512, 512) + r, RC)
            pv = jnp.dot(w_ref[slot, pl.ds(r, RC), :], kv, preferred_element_type=jnp.float32)
            acc_ref[rows, :] = acc_ref[rows, :] * f_ref[slot, pl.ds(r, RC), :] + pv

    stage1(0)
    stage2(0)
    stage1(1)

    def body(i, carry):
        stage3(i)
        stage2(i + 1)
        stage1(i + 2)
        return carry

    lax.fori_loop(0, N_UNITS - 2, body, 0)
    stage3(N_UNITS - 2)
    stage2(N_UNITS - 1)
    stage3(N_UNITS - 1)


MESH = pl.DeviceIdType.MESH


def kernel(
    tok_hbm, wq_hbm, wk_hbm, wv_hbm, bias_hbm, wo_hbm, o_ref,
    tok, wq, wk, wv, bias, wo, qs, kvs, qp, q, kv, ob, at,
    mask_ref, tri_ref, sp_ref, ls_ref, w_ref, f_ref, acc_ref,
    loc, tok_s, tok_r, w_s, w_r, wo_s, wo_r, wos_s, wos_r,
    q_s, q_r, ya_s, ya_r, zr_s, zr_r, zl_s, zl_r, sib_s, sib_r, ex_s, ex_r,
):
    sp, tp = lax.axis_index("sp"), lax.axis_index("tp")
    z, y, x, c = sp // 4, sp % 4, tp // 2, tp % 2
    zm = 7 - z

    def dev(xx, yy, zz, cc):
        return (4 * zz + yy, 2 * xx + cc)

    def remote(src, dst, s, r, to):
        return pltpu.make_async_remote_copy(
            src_ref=src, dst_ref=dst, send_sem=s, recv_sem=r, device_id=to, device_id_type=MESH
        )

    sib = dev(x, y, z, 1 - c)
    right, left = dev(x, y, (z + 1) % 8, c), dev(x, y, (z + 7) % 8, c)

    locals_ = [
        pltpu.make_async_copy(a, b, loc.at[i])
        for i, (a, b) in enumerate(
            [(tok_hbm, tok.at[x]), (wq_hbm, wq.at[c]), (wk_hbm, wk.at[c]), (wv_hbm, wv.at[c]),
             (bias_hbm, bias.at[c]), (wo_hbm, wo.at[tp])]
        )
    ]
    for cp in locals_:
        cp.start()

    barrier = pltpu.get_barrier_semaphore()
    for dx in range(4):
        for dy in range(4):
            if dx or dy:
                pl.semaphore_signal(barrier, inc=1, device_id=dev((x + dx) % 4, (y + dy) % 4, z, c), device_id_type=MESH)
            pl.semaphore_signal(barrier, inc=1, device_id=dev((x + dx) % 4, (y + dy) % 4, zm, c), device_id_type=MESH)
    for to in (sib, right, left):
        pl.semaphore_signal(barrier, inc=1, device_id=to, device_id_type=MESH)
    pl.semaphore_wait(barrier, 34)

    sends = []
    for d in (1, 3, 2):
        cp = remote(tok_hbm, tok.at[x], tok_s.at[d], tok_r.at[x], dev((x + d) % 4, y, z, c))
        cp.start()
        sends.append(cp)
    for i, (a, b) in enumerate([(wq_hbm, wq), (wk_hbm, wk), (wv_hbm, wv), (bias_hbm, bias)]):
        cp = remote(a, b.at[c], w_s.at[i], w_r.at[i], sib)
        cp.start()
        sends.append(cp)
    for i, (a, b) in enumerate([(wq_hbm, wq), (wk_hbm, wk), (wv_hbm, wv), (bias_hbm, bias)]):
        remote(a, b.at[1 - c], w_s.at[i], w_r.at[i], sib).wait_recv()
    for cp in locals_:
        cp.wait()

    b2 = bias[y // 2, pl.ds(y % 2, 1), :][:, 0:1] * LOG2E
    build_tables(b2, c, mask_ref, tri_ref)
    acc_ref[...] = jnp.zeros_like(acc_ref)

    for d in (1, 3, 2):
        xs = (x + d) % 4
        remote(tok_hbm, tok.at[xs], tok_s.at[d], tok_r.at[xs], sib).wait_recv()

    for d in (1, 3, 2):
        cp = remote(wo_hbm, wo.at[tp], wo_s.at[d], wo_r.at[x], dev((x + d) % 4, y, z, c))
        cp.start()
        sends.append(cp)

    rows = tok[...].reshape(256, 2048)
    for cc in range(2):
        qq = jnp.dot(rows, wq[cc], preferred_element_type=jnp.float32) * (LOG2E / 8)
        kk = jnp.dot(rows, wk[cc], preferred_element_type=jnp.float32)
        vv = jnp.dot(rows, wv[cc], preferred_element_type=jnp.float32)
        for j in range(2):
            lanes = slice(64 * j, 64 * j + 64)
            both = jnp.concatenate([vv[:, lanes], kk[:, lanes]], axis=1).astype(jnp.bfloat16)
            kvs[2 * cc + j] = both.reshape(4, 64, 128)
            packed = jnp.concatenate([qq[:128, lanes], qq[128:, lanes]], axis=1)
            qs[2 * cc + j] = packed.astype(jnp.bfloat16)

    for d in (1, 3, 2):
        yp = (y + d) % 4
        cp = remote(kvs.at[yp], kv.at[4 * z + y, :, c], ya_s.at[d], ya_r.at[y], dev(x, yp, z, c))
        cp.start()
        sends.append(cp)
    own = pltpu.make_async_copy(kvs.at[y], kv.at[4 * z + y, :, c], loc.at[6])
    own.start()
    zq = jnp.where(y < 2, z, zm)
    for d in (1, 3, 2):
        yp = (y + d) % 4
        cp = remote(qs.at[yp], qp.at[y], q_s.at[d], q_r.at[y], dev(x, yp, zq, c))
        cp.start()
        sends.append(cp)

    @pl.when(y < 2)
    def _():
        cp = pltpu.make_async_copy(qs.at[y], qp.at[y], loc.at[7])
        cp.start()
        cp.wait()

    @pl.when(y >= 2)
    def _():
        remote(qs.at[y], qp.at[y], q_s.at[0], q_r.at[y], dev(x, y, zm, c)).start()

    own.wait()

    def piece(zz, j):
        return kv.at[4 * zz + j, :, c]

    def pass_on(zz, j):
        cp = remote(piece(zz, j), piece(zz, j), sib_s.at[4 * zz + j], sib_r.at[4 * zz + j], sib)
        cp.start()
        sends.append(cp)

    def hop(way, t, j):
        zz = (z + 8 - t) % 8 if way == 0 else (z + t) % 8
        s, r = ((zr_s, zr_r), (zl_s, zl_r))[way]
        return remote(piece(zz, j), piece(zz, j), s.at[4 * t + j], r.at[4 * t + j], (right, left)[way])

    def landed(way, t, j):
        zz = (z + 8 - t) % 8 if way == 0 else (z + t) % 8
        s, r = ((zr_s, zr_r), (zl_s, zl_r))[way]
        remote(piece(zz, j), piece(zz, j), s.at[4 * t - 4 + j], r.at[4 * t - 4 + j], (right, left)[way]).wait_recv()
        return zz

    for j in range(4):
        @pl.when(y != j)
        def _():
            remote(kvs.at[0], piece(z, j), ya_s.at[1], ya_r.at[j], sib).wait_recv()
        for way in range(2):
            cp = hop(way, 0, j)
            cp.start()
            sends.append(cp)
        pass_on(z, j)
    for t in range(1, 5):
        for j in range(4):
            for way in range(2):
                if t < 4 or way == j // 2:
                    zz = landed(way, t, j)
                    if t < 3 or (t == 3 and way == j // 2):
                        cp = hop(way, t, j)
                        cp.start()
                        sends.append(cp)
                    pass_on(zz, j)

    for j in range(4):
        @pl.when((y != j) | (y >= 2))
        def _():
            remote(qs.at[0], qp.at[j], q_s.at[0], q_r.at[j], sib).wait_recv()
        low = qp[j].astype(jnp.float32)
        nil = jnp.zeros((128, 64), jnp.float32)
        q[pl.ds(256 * j, 128), :] = jnp.concatenate([nil, low[:, :64]], axis=1).astype(jnp.bfloat16)
        q[pl.ds(256 * j + 128, 128), :] = jnp.concatenate([nil, low[:, 64:]], axis=1).astype(jnp.bfloat16)

    for d in (1, 3, 2):
        xs = (x + d) % 4
        remote(wo_hbm, wo.at[2 * xs + c], wo_s.at[d], wo_r.at[xs], sib).wait_recv()
    for xs in range(4):
        cp = remote(wo.at[2 * xs + c], wo.at[2 * xs + c], wos_s.at[xs], wos_r.at[xs], sib)
        cp.start()
        sends.append(cp)

    for zz in range(8):
        for j in range(4):
            there = kv.at[4 * zz + j, :, 1 - c]
            remote(there, there, sib_s.at[4 * zz + j], sib_r.at[4 * zz + j], sib).wait_recv()

    attend(z, q, kv, mask_ref, tri_ref, sp_ref, ls_ref, w_ref, f_ref, acc_ref)

    ob[...] = acc_ref[...].astype(jnp.bfloat16)
    hh = 4 * x + y
    for i in range(4):
        for d in range(4):
            xb = (x + d) % 4
            src = ob.at[pl.ds(256 * i + pl.multiple_of(64 * xb, 64), 64), :]
            cp = remote(src, at.at[hh], ex_s.at[4 * i + d], ex_r.at[hh], dev(xb, i, z if i < 2 else zm, c))
            if d == 0 and i < 2:
                @pl.when(y != i)
                def _():
                    cp.start()

                @pl.when(y == i)
                def _():
                    here = pltpu.make_async_copy(src, at.at[hh], loc.at[8])
                    here.start()
                    here.wait()
            else:
                cp.start()
                sends.append(cp)
    for xs in range(4):
        there = wo.at[2 * xs + 1 - c]
        remote(there, there, wos_s.at[xs], wos_r.at[xs], sib).wait_recv()
    for g in range(16):
        @pl.when((hh != g) | (y >= 2))
        def _():
            remote(ob.at[pl.ds(0, 64), :], at.at[g], ex_s.at[0], ex_r.at[g], sib).wait_recv()

    pairs = [
        jnp.concatenate([at[2 * p].astype(jnp.float32)[:, :64], at[2 * p + 1].astype(jnp.float32)[:, :64]], axis=1).astype(jnp.bfloat16)
        for p in range(8)
    ]
    every = jnp.concatenate(pairs, axis=1)
    for n in range(0, 2048, 512):
        o_ref[:, n : n + 512] = jnp.dot(
            every, wo[:, :, n : n + 512].reshape(1024, 512), preferred_element_type=jnp.float32
        ).astype(jnp.bfloat16)

    for cp in sends:
        cp.wait_send()

    @pl.when(y >= 2)
    def _():
        remote(qs.at[y], qp.at[y], q_s.at[0], q_r.at[y], dev(x, y, zm, c)).wait_send()

    for i in range(2):
        @pl.when(y != i)
        def _():
            remote(ob.at[pl.ds(0, 64), :], at.at[hh], ex_s.at[4 * i], ex_r.at[hh], sib).wait_send()


def shards(tokens, w_query, w_key, w_value, head_bias, w_out):
    bf, f32 = jnp.bfloat16, jnp.float32
    dma = pltpu.SemaphoreType.DMA
    return pl.pallas_call(
        kernel,
        out_shape=jax.ShapeDtypeStruct((64, 2048), bf),
        in_specs=[pl.BlockSpec(memory_space=pl.ANY)] * 6,
        out_specs=pl.BlockSpec(memory_space=pltpu.VMEM),
        scratch_shapes=[
            pltpu.VMEM((4, 64, 2048), bf),
            pltpu.VMEM((2, 2048, 128), bf),
            pltpu.VMEM((2, 2048, 128), bf),
            pltpu.VMEM((2, 2048, 128), bf),
            pltpu.VMEM((2, 8, 128), f32),
            pltpu.VMEM((8, 128, 2048), bf),
            pltpu.VMEM((4, 128, 128), bf),
            pltpu.VMEM((4, 4, 64, 128), bf),
            pltpu.VMEM((4, 128, 128), bf),
            pltpu.VMEM((1024, 128), bf),
            pltpu.VMEM((32, 4, 2, 64, 128), bf),
            pltpu.VMEM((1024, 128), bf),
            pltpu.VMEM((16, 64, 128), bf),
            pltpu.VMEM((3, 256, SEG), f32),
            pltpu.VMEM((SEG, SEG), bf),
            pltpu.VMEM((2, SEG, SEG), bf),
            pltpu.VMEM((2, SEG, SEG), f32),
            pltpu.VMEM((2, SEG, SEG), bf),
            pltpu.VMEM((2, SEG, 128), f32),
            pltpu.VMEM((1024, 128), f32),
            dma((9,)), dma((4,)), dma((4,)), dma((4,)), dma((4,)), dma((4,)), dma((4,)), dma((4,)), dma((4,)),
            dma((4,)), dma((4,)), dma((4,)), dma((4,)), dma((16,)), dma((16,)), dma((16,)), dma((16,)),
            dma((32,)), dma((32,)), dma((16,)), dma((16,)),
        ],
        compiler_params=pltpu.CompilerParams(
            vmem_limit_bytes=60 * 2**20, collective_id=0, has_side_effects=True
        ),
        name="layer",
    )(tokens, w_query, w_key, w_value, jnp.broadcast_to(jnp.pad(head_bias, (0, 6))[:, None], (8, 128)), w_out)


def solution(mesh):
    placed = (P(("sp", "tp"), None), P(None, "tp"), P(None, "tp"), P(None, "tp"), P("tp"), P("tp", None))
    return jax.shard_map(
        shards, mesh=mesh, in_specs=placed, out_specs=P(("sp", "tp"), None), check_vma=False
    )
```

time: 207 us -> 97.7 us (0.47)
  the two profiles are of different devices: /device:TPU:2 before, /device:TPU:25 now
where the time goes in v2:
time: 97.7 us; the launch traced here: 97.5 us
  Pallas kernels  94.5 us (97%)
  local copies, waits for them, and re-layouts  2.99 us (3%)
    pallas_call x1, Pallas kernels, shards(): pl.pallas_call(kernel, out_shape=jax.ShapeDtypeStruct((64, 2048), bf), in...  94.5 us

profile of v2, /device:TPU:25, one launch (start us, length us, event | category | flops | bytes accessed | tf_op | source)
XLA Modules:
  0.0 97.5 jit_solution(17207738450643192728)
XLA Ops:
  0.0 0.7 pad.4
  0.7 0.7 broadcast_in_dim.2.bias_hbm
  1.3 94.5 %layer.1 = bf16[64,2048]{1,0:T(8,128)(2,1)} custom-call(bf16[64,2048]{1,0:T(8,128)(2,1)} %tok_hbm.1, bf16[2048,128]{1,0:T(8,128)(2,1)} %wq_hbm.1, bf16[2048,128]{1,0:T(8,128)(2,1)} %wk_hbm.1, bf16[2048,128]{1,0:T(8,128)(2,1)} %wv_hbm.1, f32[8,128]{1,0:T(8,128)} %broadcast_in_dim.2.bias_hbm, bf16[128,2048]{1,0:T(8,128)(2,1)} %wo_hbm.1), custom_call_target="tpu_custom_call" | custom-call | tf_op jit(solution)/shard_map/layer/pallas_call | solution.py:312
  95.9 1.7 %copy.8 = bf16[64,2048]{1,0:T(8,128)(2,1)} copy(bf16[64,2048]{1,0:T(8,128)(2,1)} %layer.1) | data formatting | bytes 524288

commit v3 on v2

v3 whole, which is shorter than its diff:
```python
import jax, jax.numpy as jnp
from jax import lax
from jax.sharding import PartitionSpec as P
from jax.experimental import pallas as pl
from jax.experimental.pallas import tpu as pltpu

LOG2E = 1.4426950408889634
SEG = 512
N_UNITS = 34
WO_ON, WO_SHARE = 14, 24
ORDER = (0, 7, 1, 6, 2, 5, 3, 4)
NEG = -1e30

def build_tables(bias2, c, mask_ref, tri_ref):
    rows = lax.broadcasted_iota(jnp.int32, (256, SEG), 0)
    cols = lax.broadcasted_iota(jnp.int32, (256, SEG), 1)
    qpos = (2 * (rows // 64) + c) * 64 + rows % 64
    mask_ref[0] = jnp.full((256, SEG), bias2, jnp.float32)
    mask_ref[1] = jnp.where(cols < qpos, bias2, NEG)
    mask_ref[2] = jnp.full((256, SEG), NEG, jnp.float32)
    j = lax.broadcasted_iota(jnp.int32, (SEG, SEG), 0)
    s = lax.broadcasted_iota(jnp.int32, (SEG, SEG), 1)
    tri_ref[...] = jnp.where(j > s, -1.0, 0.0).astype(jnp.bfloat16)

def attend(z, arrive, take_q, q_ref, kv_ref, mask_ref, tri_ref, sp_ref, ls_ref, w_ref, f_ref, acc_ref, fac_ref, RC=128):
    zm = 7 - z
    parts = []
    start = 0
    for k in range(8):
        zz = (z + ORDER[k]) % 8
        a = 4 * (zz < z).astype(jnp.int32) + 2 * (zz == z).astype(jnp.int32)
        parts.append((start, zz, a))
        start = start + a + 4 * (zz <= zm).astype(jnp.int32)

    def place(n):
        base, zz, a = parts[0]
        step = 0
        for k in range(1, 8):
            at_k = n >= parts[k][0]
            base = jnp.where(at_k, parts[k][0], base)
            zz = jnp.where(at_k, parts[k][1], zz)
            a = jnp.where(at_k, parts[k][2], a)
            step = jnp.where(at_k, (k + 1) // 2, step)
        i = n - base
        is_b = (i >= a).astype(jnp.int32)
        s = 4 * zz + i - is_b * a
        first = is_b * (4 * zm + 2) + (1 - is_b) * (4 * z)
        return (is_b, s, first, is_b * 8 + zz), step

    def stage1(n, unit):
        is_b, s, first, _ = unit
        slot = n % 2
        kv = kv_ref[s].reshape(SEG, 128)
        for r in range(0, 512, RC):
            b = first + r // 256
            idx = (s >= b).astype(jnp.int32) + (s > b).astype(jnp.int32)
            q = q_ref[pl.ds(pl.multiple_of(is_b * 512, 512) + r, RC), :]
            sc = lax.dot_general(q, kv, (((1,), (1,)), ((), ())), preferred_element_type=jnp.float32)
            sc = sc + mask_ref[idx, pl.ds(r % 256, RC), :]
            l = jnp.log2(1.0 + jnp.exp2(jnp.minimum(sc, 126.0)))
            sp = jnp.maximum(l, sc)
            sp_ref[slot, pl.ds(r, RC), :] = sp.astype(jnp.bfloat16)
            ls_ref[slot, pl.ds(r, RC), :] = sc - sp

    def stage2(n):
        slot = n % 2
        for r in range(0, 512, RC):
            sp = sp_ref[slot, pl.ds(r, RC), :]
            lo = jnp.dot(sp, tri_ref[:, 0:256], preferred_element_type=jnp.float32)
            hi = jnp.dot(sp[:, 256:], tri_ref[256:, 256:], preferred_element_type=jnp.float32)
            w_ref[slot, pl.ds(r, RC), 0:256] = jnp.exp2(ls_ref[slot, pl.ds(r, RC), 0:256] + lo).astype(jnp.bfloat16)
            w_ref[slot, pl.ds(r, RC), 256:512] = jnp.exp2(ls_ref[slot, pl.ds(r, RC), 256:512] + hi).astype(jnp.bfloat16)
            keep = lo[:, 0:1] - sp[:, 0:1].astype(jnp.float32)
            f_ref[slot, pl.ds(r, RC), :] = jnp.exp2(jnp.broadcast_to(keep, (RC, 128)))

    def stage3(n, unit):
        _, s, _, at = unit
        slot = n % 2
        kv = kv_ref[s].reshape(SEG, 128)
        for r in range(0, 512, RC):
            rows = pl.ds(r, RC)
            pv = jnp.dot(w_ref[slot, rows, :], kv, preferred_element_type=jnp.float32)
            f = f_ref[slot, rows, :]
            acc_ref[at, rows, :] = acc_ref[at, rows, :] * f + pv
            fac_ref[at, rows, :] = fac_ref[at, rows, :] * f

    u0, _ = place(0)
    u1, step = place(1)
    done, sib_done = arrive(1, step, 6, 0)
    stage1(0, u0)
    stage2(0)
    stage1(1, u1)
    take_q(2)
    take_q(3)

    def body(i, carry):
        done, sib_done, ua, ub = carry
        uc, step = place(i + 2)
        done, sib_done = arrive(i + 2, step, done, sib_done)
        stage3(i, ua)
        stage2(i + 1)
        stage1(i + 2, uc)
        return done, sib_done, ub, uc

    done, sib_done, ua, ub = lax.fori_loop(0, N_UNITS - 2, body, (done, sib_done, u0, u1))
    arrive(N_UNITS, 4, done, sib_done)
    stage3(N_UNITS - 2, ua)
    stage2(N_UNITS - 1)
    stage3(N_UNITS - 1, ub)


MESH = pl.DeviceIdType.MESH


def kernel(
    tok_hbm, wq_hbm, wk_hbm, wv_hbm, bias_hbm, wo_hbm, o_ref,
    tok, wq, wk, wv, bias, wo, qs, kvs, qp, q, kv, ob, at,
    mask_ref, tri_ref, sp_ref, ls_ref, w_ref, f_ref, acc_ref, fac_ref,
    loc, own_s, ownq_s, tok_s, tok_r, w_s, w_r, wo_s, wo_r, wos_s, wos_r,
    q_s, q_r, ya_s, ya_r, zr_s, zr_r, zl_s, zl_r, sib_s, sib_r, ex_s, ex_r,
):
    sp, tp = lax.axis_index("sp"), lax.axis_index("tp")
    z, y, x, c = sp // 4, sp % 4, tp // 2, tp % 2
    zm = 7 - z

    def dev(xx, yy, zz, cc):
        return (4 * zz + yy, 2 * xx + cc)

    def remote(src, dst, s, r, to):
        return pltpu.make_async_remote_copy(
            src_ref=src, dst_ref=dst, send_sem=s, recv_sem=r, device_id=to, device_id_type=MESH
        )

    sib = dev(x, y, z, 1 - c)
    right, left = dev(x, y, (z + 1) % 8, c), dev(x, y, (z + 7) % 8, c)

    locals_ = [
        pltpu.make_async_copy(a, b, loc.at[i])
        for i, (a, b) in enumerate(
            [(tok_hbm, tok.at[x]), (wq_hbm, wq.at[c]), (wk_hbm, wk.at[c]), (wv_hbm, wv.at[c]),
             (bias_hbm, bias.at[c]), (wo_hbm, wo.at[tp])]
        )
    ]
    for cp in locals_:
        cp.start()

    barrier = pltpu.get_barrier_semaphore()
    for dx in range(4):
        for dy in range(4):
            if dx or dy:
                pl.semaphore_signal(barrier, inc=1, device_id=dev((x + dx) % 4, (y + dy) % 4, z, c), device_id_type=MESH)
            pl.semaphore_signal(barrier, inc=1, device_id=dev((x + dx) % 4, (y + dy) % 4, zm, c), device_id_type=MESH)
    for to in (sib, right, left):
        pl.semaphore_signal(barrier, inc=1, device_id=to, device_id_type=MESH)
    pl.semaphore_wait(barrier, 34)

    x_right, x_left = dev((x + 1) % 4, y, z, c), dev((x + 3) % 4, y, z, c)
    around = (x, (x + 3) % 4, (x + 1) % 4, (x + 2) % 4)
    halves = (pl.ds(0, 32), pl.ds(32, 32))
    sends = []

    def go(cp):
        cp.start()
        sends.append(cp)

    for i in range(2):
        go(remote(tok_hbm.at[halves[i]], tok.at[x, halves[i]], tok_s.at[i], tok_r.at[2 + i], x_right))
        go(remote(tok_hbm.at[halves[1 - i]], tok.at[x, halves[1 - i]], tok_s.at[3 - i], tok_r.at[5 - i], x_left))
    shared = [(wq_hbm, wq), (wk_hbm, wk), (wv_hbm, wv), (bias_hbm, bias)]
    for i, (a, b) in enumerate(shared):
        go(remote(a, b.at[c], w_s.at[i], w_r.at[i], sib))

    acc_ref[...] = jnp.zeros_like(acc_ref)
    fac_ref[...] = jnp.ones_like(fac_ref)
    for i, (a, b) in enumerate(shared):
        remote(a, b.at[1 - c], w_s.at[i], w_r.at[i], sib).wait_recv()
    for cp in locals_:
        cp.wait()

    def tok_landed(o, i):
        there = tok.at[around[o], halves[i]]
        remote(there, there, tok_s.at[0], tok_r.at[2 * o + i], sib).wait_recv()

    def tok_on(o, i):
        there = tok.at[around[o], halves[i]]
        go(remote(there, there, tok_s.at[3 + o], tok_r.at[6 + i], x_right if o == 1 else x_left))

    zq = jnp.where(y < 2, z, zm)

    def own_q(o):
        xb = around[o]

        @pl.when(y < 2)
        def _():
            pltpu.make_async_copy(qs.at[y, xb], qp.at[y, xb], ownq_s.at[o]).start()

        @pl.when(y >= 2)
        def _():
            remote(qs.at[y, xb], qp.at[y, xb], q_s.at[4 * o], q_r.at[4 * y + o], dev(x, y, zm, c)).start()

    def project(o):
        xb = around[o]
        rows = tok[xb]
        for cc in range(2):
            qq = jnp.dot(rows, wq[cc], preferred_element_type=jnp.float32) * (LOG2E / 8)
            kk = jnp.dot(rows, wk[cc], preferred_element_type=jnp.float32)
            vv = jnp.dot(rows, wv[cc], preferred_element_type=jnp.float32)
            for j in range(2):
                lanes = slice(64 * j, 64 * j + 64)
                kvs[2 * cc + j, xb] = jnp.concatenate([vv[:, lanes], kk[:, lanes]], axis=1).astype(jnp.bfloat16)
                qs[2 * cc + j, xb] = jnp.concatenate([qq[:32, lanes], qq[32:, lanes]], axis=1).astype(jnp.bfloat16)
        for d in (1, 3, 2):
            yp = (y + d) % 4
            go(remote(qs.at[yp, xb], qp.at[y, xb], q_s.at[4 * o + d], q_r.at[4 * y + o], dev(x, yp, zq, c)))
        own_q(o)
        for d in (1, 3, 2):
            yp = (y + d) % 4
            go(remote(kvs.at[yp, xb], kv.at[4 * z + y, xb, c], ya_s.at[4 * o + d], ya_r.at[4 * o + y], dev(x, yp, z, c)))
        pltpu.make_async_copy(kvs.at[y, xb], kv.at[4 * z + y, xb, c], own_s.at[o]).start()

    def piece(zz, o):
        return kv.at[pl.ds(4 * zz, 4), row_of(o), c]

    def row_of(o):
        if isinstance(o, int):
            return around[o]
        return (x + jnp.where(o == 0, 0, jnp.where(o == 1, 3, o - 1))) % 4

    def pass_on(zz, o):
        return remote(piece(zz, o), piece(zz, o), sib_s.at[4 * zz + o], sib_r.at[4 * zz + o], sib)

    def source(way, t):
        return (z + 8 - t) % 8 if way == 0 else (z + t) % 8

    def hop(way, t, o, landing=0):
        zz = source(way, t + landing)
        s, r = ((zr_s, zr_r), (zl_s, zl_r))[way]
        return remote(piece(zz, o), piece(zz, o), s.at[4 * t + o], r.at[4 * t + o], (right, left)[way])

    def start_z(o):
        for d in (1, 3, 2):
            ys = (y + d) % 4
            there = kv.at[4 * z + ys, around[o], c]
            remote(there, there, ya_s.at[0], ya_r.at[4 * o + ys], sib).wait_recv()
        pltpu.make_async_copy(kvs.at[y, around[o]], kv.at[4 * z + y, around[o], c], own_s.at[o]).wait()
        for way in range(2):
            go(hop(way, 0, o))
        go(pass_on(z, o))

    project(0)
    tok_landed(1, 0)
    tok_on(1, 0)
    tok_landed(2, 1)
    tok_on(2, 1)
    both = bias[y // 2]
    b2 = jnp.where(y % 2 == 0, both[:, 0:1], both[:, 1:2]) * LOG2E
    start_z(0)
    tok_landed(1, 1)
    project(1)
    tok_landed(2, 0)
    project(2)
    start_z(1)
    tok_landed(3, 0)
    tok_landed(3, 1)
    project(3)
    go(remote(wo_hbm, wo.at[tp], wo_s.at[0], wo_r.at[2], x_right))
    go(remote(wo_hbm, wo.at[tp], wo_s.at[1], wo_r.at[4], x_left))
    build_tables(b2, c, mask_ref, tri_ref)
    def take_q(j):
        @pl.when((y == j) & (y < 2))
        def _():
            for o in range(4):
                pltpu.make_async_copy(qs.at[y, 0], qp.at[y, 0], ownq_s.at[o]).wait()

        @pl.when((y != j) | (y >= 2))
        def _():
            for o in range(4):
                remote(qs.at[0, 0], qp.at[j, around[o]], q_s.at[0], q_r.at[4 * j + o], sib).wait_recv()
        for xb in range(4):
            low = qp[j, xb].astype(jnp.float32)
            nil = jnp.zeros((32, 64), jnp.float32)
            at_row = 256 * j + 64 * xb
            q[pl.ds(at_row, 32), :] = jnp.concatenate([nil, low[:, :64]], axis=1).astype(jnp.bfloat16)
            q[pl.ds(at_row + 32, 32), :] = jnp.concatenate([nil, low[:, 64:]], axis=1).astype(jnp.bfloat16)

    wo_half = (pl.ds(0, 64), pl.ds(64, 64))

    def wo_hop(o, i):
        there = wo.at[2 * around[o] + c, wo_half[i]]
        return remote(there, there, wo_s.at[1 + o], wo_r.at[6 + i], x_right if o == 1 else x_left)

    def wo_share(o):
        there = wo.at[2 * around[o] + c]
        return remote(there, there, wos_s.at[o], wos_r.at[o], sib)

    def event(e, carry):
        t, o = e // 4, e % 4
        for way in range(2):
            @pl.when((t < 4) | (o // 2 == way))
            def _():
                hop(way, t - 1, o, 1).wait_recv()

                @pl.when((t < 3) | ((t == 3) & (o // 2 == way)))
                def _():
                    hop(way, t, o).start()
                pass_on(source(way, t), o).start()
        return carry

    def sib_event(e, carry):
        t, o = e // 4, e % 4

        def wait_for(zz):
            there = kv.at[pl.ds(4 * zz, 4), row_of(o), 1 - c]
            remote(there, there, sib_s.at[0], sib_r.at[4 * zz + o], sib).wait_recv()

        wait_for(source(0, t))

        @pl.when((t > 0) & (t < 4))
        def _():
            wait_for(source(1, t))
        return carry

    start_z(2)
    event(4, 0)
    take_q(0)
    take_q(1)
    start_z(3)
    event(5, 0)

    def arrive(n, step, done, sib_done):
        need = 4 * step + 4
        upto = jnp.maximum(need, jnp.minimum(20, 6 + n * 2 // 3))
        lax.fori_loop(done, upto, event, 0)
        done = jnp.maximum(done, upto)
        lax.fori_loop(sib_done, need, sib_event, 0)
        sib_done = jnp.maximum(sib_done, need)

        @pl.when(n == WO_ON)
        def _():
            for o in (1, 2):
                there = wo.at[2 * around[o] + c]
                remote(there, there, wo_s.at[0], wo_r.at[2 * o], sib).wait_recv()
                wo_hop(o, o - 1).start()

        @pl.when(n == WO_SHARE)
        def _():
            for i in range(2):
                there = wo.at[2 * around[3] + c, wo_half[i]]
                remote(there, there, wo_s.at[0], wo_r.at[6 + i], sib).wait_recv()
            for o in range(4):
                wo_share(o).start()
        return done, sib_done

    attend(z, arrive, take_q, q, kv, mask_ref, tri_ref, sp_ref, ls_ref, w_ref, f_ref, acc_ref, fac_ref)

    for b in range(2):
        for r in range(0, 512, 64):
            rows = pl.ds(r, 64)
            total = acc_ref[8 * b, rows, :]
            for zz in range(1, 8):
                total = total * fac_ref[8 * b + zz, rows, :] + acc_ref[8 * b + zz, rows, :]
            ob[pl.ds(512 * b + r, 64), :] = total.astype(jnp.bfloat16)
    hh = 4 * x + y
    for i in range(4):
        for d in range(4):
            xb = (x + d) % 4
            src = ob.at[pl.ds(256 * i + pl.multiple_of(64 * xb, 64), 64), :]
            cp = remote(src, at.at[hh], ex_s.at[4 * i + d], ex_r.at[hh], dev(xb, i, z if i < 2 else zm, c))
            if d == 0 and i < 2:
                @pl.when(y != i)
                def _():
                    cp.start()

                @pl.when(y == i)
                def _():
                    here = pltpu.make_async_copy(src, at.at[hh], loc.at[8])
                    here.start()
                    here.wait()
            else:
                cp.start()
                sends.append(cp)
    for o in range(4):
        there = wo.at[2 * around[o] + 1 - c]
        remote(there, there, wos_s.at[o], wos_r.at[o], sib).wait_recv()
    for g in range(16):
        @pl.when((hh != g) | (y >= 2))
        def _():
            remote(ob.at[pl.ds(0, 64), :], at.at[g], ex_s.at[0], ex_r.at[g], sib).wait_recv()

    pairs = [
        jnp.concatenate([at[2 * p].astype(jnp.float32)[:, :64], at[2 * p + 1].astype(jnp.float32)[:, :64]], axis=1).astype(jnp.bfloat16)
        for p in range(8)
    ]
    every = jnp.concatenate(pairs, axis=1)
    for n in range(0, 2048, 512):
        o_ref[:, n : n + 512] = jnp.dot(
            every, wo[:, :, n : n + 512].reshape(1024, 512), preferred_element_type=jnp.float32
        ).astype(jnp.bfloat16)

    for cp in sends:
        cp.wait_send()
    for o in range(4):
        wo_share(o).wait_send()
    for o in (1, 2):
        wo_hop(o, o - 1).wait_send()
    for t in range(1, 5):
        for o in range(4):
            for way in range(2):
                if t < 4 or o // 2 == way:
                    if t < 3 or (t == 3 and o // 2 == way):
                        hop(way, t, o).wait_send()
                    pass_on(source(way, t), o).wait_send()

    @pl.when(y >= 2)
    def _():
        for o in range(4):
            remote(qs.at[y, 0], qp.at[y, 0], q_s.at[4 * o], q_r.at[0], dev(x, y, zm, c)).wait_send()

    for i in range(2):
        @pl.when(y != i)
        def _():
            remote(ob.at[pl.ds(0, 64), :], at.at[hh], ex_s.at[4 * i], ex_r.at[hh], sib).wait_send()


def shards(tokens, w_query, w_key, w_value, head_bias, w_out):
    bf, f32 = jnp.bfloat16, jnp.float32
    dma = pltpu.SemaphoreType.DMA
    return pl.pallas_call(
        kernel,
        out_shape=jax.ShapeDtypeStruct((64, 2048), bf),
        in_specs=[pl.BlockSpec(memory_space=pl.ANY)] * 6,
        out_specs=pl.BlockSpec(memory_space=pltpu.VMEM),
        scratch_shapes=[
            pltpu.VMEM((4, 64, 2048), bf),
            pltpu.VMEM((2, 2048, 128), bf),
            pltpu.VMEM((2, 2048, 128), bf),
            pltpu.VMEM((2, 2048, 128), bf),
            pltpu.VMEM((2, 1, 2), f32),
            pltpu.VMEM((8, 128, 2048), bf),
            pltpu.VMEM((4, 4, 32, 128), bf),
            pltpu.VMEM((4, 4, 64, 128), bf),
            pltpu.VMEM((4, 4, 32, 128), bf),
            pltpu.VMEM((1024, 128), bf),
            pltpu.VMEM((32, 4, 2, 64, 128), bf),
            pltpu.VMEM((1024, 128), bf),
            pltpu.VMEM((16, 64, 128), bf),
            pltpu.VMEM((3, 256, SEG), f32),
            pltpu.VMEM((SEG, SEG), bf),
            pltpu.VMEM((2, SEG, SEG), bf),
            pltpu.VMEM((2, SEG, SEG), f32),
            pltpu.VMEM((2, SEG, SEG), bf),
            pltpu.VMEM((2, SEG, 128), f32),
            pltpu.VMEM((16, SEG, 128), f32),
            pltpu.VMEM((16, SEG, 128), f32),
            dma((9,)), dma((4,)), dma((4,)), dma((6,)), dma((8,)), dma((4,)), dma((4,)), dma((4,)), dma((8,)), dma((4,)),
            dma((4,)), dma((16,)), dma((16,)), dma((16,)), dma((16,)), dma((16,)), dma((16,)), dma((16,)), dma((16,)),
            dma((32,)), dma((32,)), dma((16,)), dma((16,)),
        ],
        compiler_params=pltpu.CompilerParams(
            vmem_limit_bytes=60 * 2**20, collective_id=0, has_side_effects=True
        ),
        name="layer",
    )(tokens, w_query, w_key, w_value, head_bias.reshape(1, 2), w_out)


def solution(mesh):
    placed = (P(("sp", "tp"), None), P(None, "tp"), P(None, "tp"), P(None, "tp"), P("tp"), P("tp", None))
    return jax.shard_map(
        shards, mesh=mesh, in_specs=placed, out_specs=P(("sp", "tp"), None), check_vma=False
    )
```

time: 97.7 us -> 77.8 us (0.80)
  Pallas kernels: 94.5 us -> 76 us
  local copies, waits for them, and re-layouts: 2.99 us -> 1.67 us
    pallas_call x1, Pallas kernels: 94.5 us -> 76 us  [shards(): pl.pallas_call(kernel, out_shape=jax.ShapeDtypeStruct((64, 2048), bf), in...]
where the time goes in v3:
time: 77.8 us; the launch traced here: 77.7 us
  Pallas kernels  76 us (98%)
  local copies, waits for them, and re-layouts  1.67 us (2%)
    pallas_call x1, Pallas kernels, shards(): pl.pallas_call(kernel, out_shape=jax.ShapeDtypeStruct((64, 2048), bf), in...  76 us
    unnamed x1, local copies, waits for them, and re-layouts  1.67 us

profile of v3, /device:TPU:25, one launch (start us, length us, event | category | flops | bytes accessed | tf_op | source)
XLA Modules:
  0.0 77.7 jit_solution(15477174315204106264)
XLA Ops:
  0.0 76.0 %layer.1 = bf16[64,2048]{1,0:T(8,128)(2,1)} custom-call(bf16[64,2048]{1,0:T(8,128)(2,1)} %tok_hbm.1, bf16[2048,128]{1,0:T(8,128)(2,1)} %wq_hbm.1, bf16[2048,128]{1,0:T(8,128)(2,1)} %wk_hbm.1, bf16[2048,128]{1,0:T(8,128)(2,1)} %wv_hbm.1, f32[1,2]{1,0:T(1,128)} %bitcast.1, bf16[128,2048]{1,0:T(8,128)(2,1)} %wo_hbm.1), custom_call_target="tpu_custom_call" | custom-call | tf_op jit(solution)/shard_map/layer/pallas_call | solution.py:428
  76.0 1.7 %copy.8 = bf16[64,2048]{1,0:T(8,128)(2,1)} copy(bf16[64,2048]{1,0:T(8,128)(2,1)} %layer.1) | data formatting | bytes 524288

commit v4 on v3

--- a/solution.py
+++ b/solution.py
@@ -7,7 +7,7 @@
 LOG2E = 1.4426950408889634
 SEG = 512
 N_UNITS = 34
-WO_ON, WO_SHARE = 14, 24
+WO_ON, WO_SHARE = 6, 11
 ORDER = (0, 7, 1, 6, 2, 5, 3, 4)
 NEG = -1e30
 
@@ -29,27 +29,28 @@
     for k in range(8):
         zz = (z + ORDER[k]) % 8
         a = 4 * (zz < z).astype(jnp.int32) + 2 * (zz == z).astype(jnp.int32)
-        parts.append((start, zz, a))
-        start = start + a + 4 * (zz <= zm).astype(jnp.int32)
+        b = 4 * (zz <= zm).astype(jnp.int32)
+        parts.append((start, zz, a if k == 0 else 0, b))
+        start = start + a + b
 
     def place(n):
-        base, zz, a = parts[0]
+        base, zz, lo, b = parts[0]
         step = 0
         for k in range(1, 8):
             at_k = n >= parts[k][0]
             base = jnp.where(at_k, parts[k][0], base)
             zz = jnp.where(at_k, parts[k][1], zz)
-            a = jnp.where(at_k, parts[k][2], a)
+            lo = jnp.where(at_k, parts[k][2], lo)
+            b = jnp.where(at_k, parts[k][3], b)
             step = jnp.where(at_k, (k + 1) // 2, step)
         i = n - base
-        is_b = (i >= a).astype(jnp.int32)
-        s = 4 * zz + i - is_b * a
+        is_b = ((i >= lo) & (i < lo + b)).astype(jnp.int32)
+        s = 4 * zz + i - jnp.where(is_b == 1, lo, jnp.where(i < lo, 0, b))
         first = is_b * (4 * zm + 2) + (1 - is_b) * (4 * z)
         return (is_b, s, first, is_b * 8 + zz), step
 
-    def stage1(n, unit):
+    def stage1(slot, unit):
         is_b, s, first, _ = unit
-        slot = n % 2
         kv = kv_ref[s].reshape(SEG, 128)
         for r in range(0, 512, RC):
             b = first + r // 256
@@ -62,8 +63,7 @@
             sp_ref[slot, pl.ds(r, RC), :] = sp.astype(jnp.bfloat16)
             ls_ref[slot, pl.ds(r, RC), :] = sc - sp
 
-    def stage2(n):
-        slot = n % 2
+    def stage2(slot):
         for r in range(0, 512, RC):
             sp = sp_ref[slot, pl.ds(r, RC), :]
             lo = jnp.dot(sp, tri_ref[:, 0:256], preferred_element_type=jnp.float32)
@@ -73,9 +73,8 @@
             keep = lo[:, 0:1] - sp[:, 0:1].astype(jnp.float32)
             f_ref[slot, pl.ds(r, RC), :] = jnp.exp2(jnp.broadcast_to(keep, (RC, 128)))
 
-    def stage3(n, unit):
+    def stage3(slot, unit):
         _, s, _, at = unit
-        slot = n % 2
         kv = kv_ref[s].reshape(SEG, 128)
         for r in range(0, 512, RC):
             rows = pl.ds(r, RC)
@@ -86,7 +85,7 @@
 
     u0, _ = place(0)
     u1, step = place(1)
-    done, sib_done = arrive(1, step, 6, 0)
+    done, sib_done = arrive(-1, step, 7, 0)
     stage1(0, u0)
     stage2(0)
     stage1(1, u1)
@@ -95,18 +94,22 @@
 
     def body(i, carry):
         done, sib_done, ua, ub = carry
-        uc, step = place(i + 2)
-        done, sib_done = arrive(i + 2, step, done, sib_done)
-        stage3(i, ua)
-        stage2(i + 1)
-        stage1(i + 2, uc)
-        return done, sib_done, ub, uc
-
-    done, sib_done, ua, ub = lax.fori_loop(0, N_UNITS - 2, body, (done, sib_done, u0, u1))
+        uc, _ = place(2 * i + 2)
+        ud, step = place(2 * i + 3)
+        done, sib_done = arrive(i, step, done, sib_done)
+        stage3(0, ua)
+        stage2(1)
+        stage1(0, uc)
+        stage3(1, ub)
+        stage2(0)
+        stage1(1, ud)
+        return done, sib_done, uc, ud
+
+    done, sib_done, ua, ub = lax.fori_loop(0, (N_UNITS - 2) // 2, body, (done, sib_done, u0, u1))
     arrive(N_UNITS, 4, done, sib_done)
-    stage3(N_UNITS - 2, ua)
-    stage2(N_UNITS - 1)
-    stage3(N_UNITS - 1, ub)
+    stage3(0, ua)
+    stage2(1)
+    stage3(1, ub)
 
 
 MESH = pl.DeviceIdType.MESH
@@ -326,10 +329,11 @@
     take_q(1)
     start_z(3)
     event(5, 0)
+    event(6, 0)
 
     def arrive(n, step, done, sib_done):
         need = 4 * step + 4
-        upto = jnp.maximum(need, jnp.minimum(20, 6 + n * 2 // 3))
+        upto = jnp.maximum(need, jnp.minimum(20, 9 + n * 4 // 3))
         lax.fori_loop(done, upto, event, 0)
         done = jnp.maximum(done, upto)
         lax.fori_loop(sib_done, need, sib_event, 0)
@@ -359,12 +363,14 @@
             total = acc_ref[8 * b, rows, :]
             for zz in range(1, 8):
                 total = total * fac_ref[8 * b + zz, rows, :] + acc_ref[8 * b + zz, rows, :]
-            ob[pl.ds(512 * b + r, 64), :] = total.astype(jnp.bfloat16)
+            ob[pl.ds(256 * b + r // 2, 32), :] = jnp.concatenate([total[:32, :64], total[32:, :64]], axis=1).astype(
+                jnp.bfloat16
+            )
     hh = 4 * x + y
     for i in range(4):
         for d in range(4):
             xb = (x + d) % 4
-            src = ob.at[pl.ds(256 * i + pl.multiple_of(64 * xb, 64), 64), :]
+            src = ob.at[pl.ds(128 * i + pl.multiple_of(32 * xb, 32), 32), :]
             cp = remote(src, at.at[hh], ex_s.at[4 * i + d], ex_r.at[hh], dev(xb, i, z if i < 2 else zm, c))
             if d == 0 and i < 2:
                 @pl.when(y != i)
@@ -385,13 +391,12 @@
     for g in range(16):
         @pl.when((hh != g) | (y >= 2))
         def _():
-            remote(ob.at[pl.ds(0, 64), :], at.at[g], ex_s.at[0], ex_r.at[g], sib).wait_recv()
-
-    pairs = [
-        jnp.concatenate([at[2 * p].astype(jnp.float32)[:, :64], at[2 * p + 1].astype(jnp.float32)[:, :64]], axis=1).astype(jnp.bfloat16)
-        for p in range(8)
-    ]
-    every = jnp.concatenate(pairs, axis=1)
+            remote(ob.at[pl.ds(0, 32), :], at.at[g], ex_s.at[0], ex_r.at[g], sib).wait_recv()
+
+    heads = [at[h].astype(jnp.float32) for h in range(16)]
+    upper = jnp.concatenate([head[:, :64] for head in heads], axis=1)
+    lower = jnp.concatenate([head[:, 64:] for head in heads], axis=1)
+    every = jnp.concatenate([upper, lower], axis=0).astype(jnp.bfloat16)
     for n in range(0, 2048, 512):
         o_ref[:, n : n + 512] = jnp.dot(
             every, wo[:, :, n : n + 512].reshape(1024, 512), preferred_element_type=jnp.float32
@@ -419,7 +424,7 @@
     for i in range(2):
         @pl.when(y != i)
         def _():
-            remote(ob.at[pl.ds(0, 64), :], at.at[hh], ex_s.at[4 * i], ex_r.at[hh], sib).wait_send()
+            remote(ob.at[pl.ds(0, 32), :], at.at[hh], ex_s.at[4 * i], ex_r.at[hh], sib).wait_send()
 
 
 def shards(tokens, w_query, w_key, w_value, head_bias, w_out):
@@ -442,8 +447,8 @@
             pltpu.VMEM((4, 4, 32, 128), bf),
             pltpu.VMEM((1024, 128), bf),
             pltpu.VMEM((32, 4, 2, 64, 128), bf),
-            pltpu.VMEM((1024, 128), bf),
-            pltpu.VMEM((16, 64, 128), bf),
+            pltpu.VMEM((512, 128), bf),
+            pltpu.VMEM((16, 32, 128), bf),
             pltpu.VMEM((3, 256, SEG), f32),
             pltpu.VMEM((SEG, SEG), bf),
             pltpu.VMEM((2, SEG, SEG), bf),

time: 77.8 us -> 72.9 us (0.937)
  Pallas kernels: 76 us -> 71 us
    pallas_call x1, Pallas kernels: 76 us -> 71 us  [shards(): pl.pallas_call(kernel, out_shape=jax.ShapeDtypeStruct((64, 2048), bf), in...]
where the time goes in v4:
time: 72.9 us; the launch traced here: 72.7 us
  Pallas kernels  71 us (97%)
  local copies, waits for them, and re-layouts  1.67 us (2%)
    pallas_call x1, Pallas kernels, shards(): pl.pallas_call(kernel, out_shape=jax.ShapeDtypeStruct((64, 2048), bf), in...  71 us
    unnamed x1, local copies, waits for them, and re-layouts  1.67 us

profile of v4, /device:TPU:25, one launch (start us, length us, event | category | flops | bytes accessed | tf_op | source)
XLA Modules:
  0.0 72.7 jit_solution(5201149952071719857)
XLA Ops:
  0.0 71.0 %layer.1 = bf16[64,2048]{1,0:T(8,128)(2,1)} custom-call(bf16[64,2048]{1,0:T(8,128)(2,1)} %tok_hbm.1, bf16[2048,128]{1,0:T(8,128)(2,1)} %wq_hbm.1, bf16[2048,128]{1,0:T(8,128)(2,1)} %wk_hbm.1, bf16[2048,128]{1,0:T(8,128)(2,1)} %wv_hbm.1, f32[1,2]{1,0:T(1,128)} %bitcast.1, bf16[128,2048]{1,0:T(8,128)(2,1)} %wo_hbm.1), custom_call_target="tpu_custom_call" | custom-call | tf_op jit(solution)/shard_map/layer/pallas_call | solution.py:433
  71.0 1.7 %copy.8 = bf16[64,2048]{1,0:T(8,128)(2,1)} copy(bf16[64,2048]{1,0:T(8,128)(2,1)} %layer.1) | data formatting | bytes 524288

commit v5 on v4

--- a/solution.py
+++ b/solution.py
@@ -7,7 +7,7 @@
 LOG2E = 1.4426950408889634
 SEG = 512
 N_UNITS = 34
-WO_ON, WO_SHARE = 6, 11
+WO_ON, WO_SHARE = 8, 13
 ORDER = (0, 7, 1, 6, 2, 5, 3, 4)
 NEG = -1e30
 
@@ -117,9 +117,9 @@
 
 def kernel(
     tok_hbm, wq_hbm, wk_hbm, wv_hbm, bias_hbm, wo_hbm, o_ref,
-    tok, wq, wk, wv, bias, wo, qs, kvs, qp, q, kv, ob, at,
+    tok, wq, wk, wv, bias, wo, qs, kvs, qp, q, kv, ob, at, obuf,
     mask_ref, tri_ref, sp_ref, ls_ref, w_ref, f_ref, acc_ref, fac_ref,
-    loc, own_s, ownq_s, tok_s, tok_r, w_s, w_r, wo_s, wo_r, wos_s, wos_r,
+    out_s, loc, own_s, ownq_s, tok_s, tok_r, w_s, w_r, wo_s, wo_r, wos_s, wos_r,
     q_s, q_r, ya_s, ya_r, zr_s, zr_r, zl_s, zl_r, sib_s, sib_r, ex_s, ex_r,
 ):
     sp, tp = lax.axis_index("sp"), lax.axis_index("tp")
@@ -212,11 +212,11 @@
                 lanes = slice(64 * j, 64 * j + 64)
                 kvs[2 * cc + j, xb] = jnp.concatenate([vv[:, lanes], kk[:, lanes]], axis=1).astype(jnp.bfloat16)
                 qs[2 * cc + j, xb] = jnp.concatenate([qq[:32, lanes], qq[32:, lanes]], axis=1).astype(jnp.bfloat16)
-        for d in (1, 3, 2):
+        for d in (2, 1, 3):
             yp = (y + d) % 4
             go(remote(qs.at[yp, xb], qp.at[y, xb], q_s.at[4 * o + d], q_r.at[4 * y + o], dev(x, yp, zq, c)))
         own_q(o)
-        for d in (1, 3, 2):
+        for d in (2, 1, 3):
             yp = (y + d) % 4
             go(remote(kvs.at[yp, xb], kv.at[4 * z + y, xb, c], ya_s.at[4 * o + d], ya_r.at[4 * o + y], dev(x, yp, z, c)))
         pltpu.make_async_copy(kvs.at[y, xb], kv.at[4 * z + y, xb, c], own_s.at[o]).start()
@@ -333,7 +333,7 @@
 
     def arrive(n, step, done, sib_done):
         need = 4 * step + 4
-        upto = jnp.maximum(need, jnp.minimum(20, 9 + n * 4 // 3))
+        upto = jnp.maximum(need, jnp.minimum(20, 10 + n * 4 // 3))
         lax.fori_loop(done, upto, event, 0)
         done = jnp.maximum(done, upto)
         lax.fori_loop(sib_done, need, sib_event, 0)
@@ -357,7 +357,7 @@
 
     attend(z, arrive, take_q, q, kv, mask_ref, tri_ref, sp_ref, ls_ref, w_ref, f_ref, acc_ref, fac_ref)
 
-    for b in range(2):
+    for b in (1, 0):
         for r in range(0, 512, 64):
             rows = pl.ds(r, 64)
             total = acc_ref[8 * b, rows, :]
@@ -367,8 +367,9 @@
                 jnp.bfloat16
             )
     hh = 4 * x + y
-    for i in range(4):
-        for d in range(4):
+    exits = []
+    for i in (2, 3, 0, 1):
+        for d in (2, 1, 3, 0):
             xb = (x + d) % 4
             src = ob.at[pl.ds(128 * i + pl.multiple_of(32 * xb, 32), 32), :]
             cp = remote(src, at.at[hh], ex_s.at[4 * i + d], ex_r.at[hh], dev(xb, i, z if i < 2 else zm, c))
@@ -384,24 +385,10 @@
                     here.wait()
             else:
                 cp.start()
-                sends.append(cp)
+                exits.append(cp)
     for o in range(4):
         there = wo.at[2 * around[o] + 1 - c]
         remote(there, there, wos_s.at[o], wos_r.at[o], sib).wait_recv()
-    for g in range(16):
-        @pl.when((hh != g) | (y >= 2))
-        def _():
-            remote(ob.at[pl.ds(0, 32), :], at.at[g], ex_s.at[0], ex_r.at[g], sib).wait_recv()
-
-    heads = [at[h].astype(jnp.float32) for h in range(16)]
-    upper = jnp.concatenate([head[:, :64] for head in heads], axis=1)
-    lower = jnp.concatenate([head[:, 64:] for head in heads], axis=1)
-    every = jnp.concatenate([upper, lower], axis=0).astype(jnp.bfloat16)
-    for n in range(0, 2048, 512):
-        o_ref[:, n : n + 512] = jnp.dot(
-            every, wo[:, :, n : n + 512].reshape(1024, 512), preferred_element_type=jnp.float32
-        ).astype(jnp.bfloat16)
-
     for cp in sends:
         cp.wait_send()
     for o in range(4):
@@ -421,10 +408,30 @@
         for o in range(4):
             remote(qs.at[y, 0], qp.at[y, 0], q_s.at[4 * o], q_r.at[0], dev(x, y, zm, c)).wait_send()
 
+    for g in range(16):
+        @pl.when((hh != g) | (y >= 2))
+        def _():
+            remote(ob.at[pl.ds(0, 32), :], at.at[g], ex_s.at[0], ex_r.at[g], sib).wait_recv()
+
+    heads = [at[h].astype(jnp.float32) for h in range(16)]
+    upper = jnp.concatenate([head[:, :64] for head in heads], axis=1)
+    lower = jnp.concatenate([head[:, 64:] for head in heads], axis=1)
+    every = jnp.concatenate([upper, lower], axis=0).astype(jnp.bfloat16)
+    for n in range(0, 2048, 512):
+        obuf[:, n : n + 512] = jnp.dot(
+            every, wo[:, :, n : n + 512].reshape(1024, 512), preferred_element_type=jnp.float32
+        ).astype(jnp.bfloat16)
+        pltpu.make_async_copy(obuf.at[:, n : n + 512], o_ref.at[:, n : n + 512], out_s.at[n // 512]).start()
+
+    for cp in exits:
+        cp.wait_send()
     for i in range(2):
         @pl.when(y != i)
         def _():
             remote(ob.at[pl.ds(0, 32), :], at.at[hh], ex_s.at[4 * i], ex_r.at[hh], sib).wait_send()
+
+    for n in range(0, 2048, 512):
+        pltpu.make_async_copy(obuf.at[:, n : n + 512], o_ref.at[:, n : n + 512], out_s.at[n // 512]).wait()
 
 
 def shards(tokens, w_query, w_key, w_value, head_bias, w_out):
@@ -434,7 +441,7 @@
         kernel,
         out_shape=jax.ShapeDtypeStruct((64, 2048), bf),
         in_specs=[pl.BlockSpec(memory_space=pl.ANY)] * 6,
-        out_specs=pl.BlockSpec(memory_space=pltpu.VMEM),
+        out_specs=pl.BlockSpec(memory_space=pl.ANY),
         scratch_shapes=[
             pltpu.VMEM((4, 64, 2048), bf),
             pltpu.VMEM((2, 2048, 128), bf),
@@ -449,6 +456,7 @@
             pltpu.VMEM((32, 4, 2, 64, 128), bf),
             pltpu.VMEM((512, 128), bf),
             pltpu.VMEM((16, 32, 128), bf),
+            pltpu.VMEM((64, 2048), bf),
             pltpu.VMEM((3, 256, SEG), f32),
             pltpu.VMEM((SEG, SEG), bf),
             pltpu.VMEM((2, SEG, SEG), bf),
@@ -457,7 +465,7 @@
             pltpu.VMEM((2, SEG, 128), f32),
             pltpu.VMEM((16, SEG, 128), f32),
             pltpu.VMEM((16, SEG, 128), f32),
-            dma((9,)), dma((4,)), dma((4,)), dma((6,)), dma((8,)), dma((4,)), dma((4,)), dma((4,)), dma((8,)), dma((4,)),
+            dma((4,)), dma((9,)), dma((4,)), dma((4,)), dma((6,)), dma((8,)), dma((4,)), dma((4,)), dma((4,)), dma((8,)), dma((4,)),
             dma((4,)), dma((16,)), dma((16,)), dma((16,)), dma((16,)), dma((16,)), dma((16,)), dma((16,)), dma((16,)),
             dma((32,)), dma((32,)), dma((16,)), dma((16,)),
         ],

time: 72.9 us -> 72.2 us (level)
  Pallas kernels: 71 us -> 69.6 us
    pallas_call x1, Pallas kernels: 71 us -> 69.6 us  [shards(): pl.pallas_call(kernel, out_shape=jax.ShapeDtypeStruct((64, 2048), bf), in...]
where the time goes in v5:
time: 72.2 us; the launch traced here: 71.3 us
  Pallas kernels  69.6 us (96%)
  local copies, waits for them, and re-layouts  1.67 us (2%)
    pallas_call x1, Pallas kernels, shards(): pl.pallas_call(kernel, out_shape=jax.ShapeDtypeStruct((64, 2048), bf), in...  69.6 us
    unnamed x1, local copies, waits for them, and re-layouts  1.67 us

profile of v5, /device:TPU:25, one launch (start us, length us, event | category | flops | bytes accessed | tf_op | source)
XLA Modules:
  0.0 71.3 jit_solution(10184048630092179287)
XLA Ops:
  0.0 69.6 %layer.1 = bf16[64,2048]{1,0:T(8,128)(2,1)} custom-call(bf16[64,2048]{1,0:T(8,128)(2,1)} %tok_hbm.1, bf16[2048,128]{1,0:T(8,128)(2,1)} %wq_hbm.1, bf16[2048,128]{1,0:T(8,128)(2,1)} %wk_hbm.1, bf16[2048,128]{1,0:T(8,128)(2,1)} %wv_hbm.1, f32[1,2]{1,0:T(1,128)} %bitcast.1, bf16[128,2048]{1,0:T(8,128)(2,1)} %wo_hbm.1), custom_call_target="tpu_custom_call" | custom-call | tf_op jit(solution)/shard_map/layer/pallas_call | solution.py:440
  69.6 1.7 %copy.8 = bf16[64,2048]{1,0:T(8,128)(2,1)} copy(bf16[64,2048]{1,0:T(8,128)(2,1)} %layer.1) | data formatting | bytes 524288

commit v6 on v5

--- a/solution.py
+++ b/solution.py
@@ -470,7 +470,7 @@
             dma((32,)), dma((32,)), dma((16,)), dma((16,)),
         ],
         compiler_params=pltpu.CompilerParams(
-            vmem_limit_bytes=60 * 2**20, collective_id=0, has_side_effects=True
+            vmem_limit_bytes=36 * 2**20, collective_id=0, has_side_effects=True
         ),
         name="layer",
     )(tokens, w_query, w_key, w_value, head_bias.reshape(1, 2), w_out)

time: 72.2 us -> 77 us (1.066)
  local copies, waits for them, and re-layouts: 1.67 us -> 6.47 us
    unnamed x1 -> x13, local copies, waits for them, and re-layouts: 1.67 us -> 6.47 us
where the time goes in v6:
time: 77 us; the launch traced here: 75.9 us
  Pallas kernels  69.4 us (90%)
  local copies, waits for them, and re-layouts  6.47 us (8%)
    pallas_call x1, Pallas kernels, shards(): pl.pallas_call(kernel, out_shape=jax.ShapeDtypeStruct((64, 2048), bf), in...  69.4 us
    unnamed x13, local copies, waits for them, and re-layouts  6.47 us

profile of v6, /device:TPU:25, one launch (start us, length us, event | category | flops | bytes accessed | tf_op | source)
XLA Modules:
  0.0 75.9 jit_solution(15923261286588401889)
XLA Ops:
  0.0 0.0 copy-start.5
  0.0 0.7 copy-done.5
  0.7 0.0 copy-start
  0.7 1.0 %copy-done = bf16[2048,128]{1,0:T(8,128)(2,1)S(1)} copy-done((bf16[2048,128]{1,0:T(8,128)(2,1)S(1)}, bf16[2048,128]{1,0:T(8,128)(2,1)}, u32[]{:S(2)}) %copy-start) | copy-done | bytes 524312
  1.7 0.0 copy-start.1
  1.7 1.0 %copy-done.1 = bf16[2048,128]{1,0:T(8,128)(2,1)S(1)} copy-done((bf16[2048,128]{1,0:T(8,128)(2,1)S(1)}, bf16[2048,128]{1,0:T(8,128)(2,1)}, u32[]{:S(2)}) %copy-start.1) | copy-done | bytes 524312
  2.7 0.0 copy-start.2
  2.7 1.0 %copy-done.2 = bf16[2048,128]{1,0:T(8,128)(2,1)S(1)} copy-done((bf16[2048,128]{1,0:T(8,128)(2,1)S(1)}, bf16[2048,128]{1,0:T(8,128)(2,1)}, u32[]{:S(2)}) %copy-start.2) | copy-done | bytes 524312
  3.8 0.0 copy-start.3
  3.8 1.0 %copy-done.3 = bf16[128,2048]{1,0:T(8,128)(2,1)S(1)} copy-done((bf16[128,2048]{1,0:T(8,128)(2,1)S(1)}, bf16[128,2048]{1,0:T(8,128)(2,1)}, u32[]{:S(2)}) %copy-start.3) | copy-done | bytes 524312
  4.8 0.0 copy-start.4
  4.8 0.9 %copy-done.4 = bf16[64,2048]{1,0:T(8,128)(2,1)S(1)} copy-done((bf16[64,2048]{1,0:T(8,128)(2,1)S(1)}, bf16[64,2048]{1,0:T(8,128)(2,1)}, u32[]{:S(2)}) %copy-start.4) | copy-done | bytes 262168
  5.8 69.4 %layer.1 = bf16[64,2048]{1,0:T(8,128)(2,1)S(1)} custom-call(bf16[64,2048]{1,0:T(8,128)(2,1)S(1)} %copy-done.4, bf16[2048,128]{1,0:T(8,128)(2,1)S(1)} %copy-done, bf16[2048,128]{1,0:T(8,128)(2,1)S(1)} %copy-done.1, bf16[2048,128]{1,0:T(8,128)(2,1)S(1)} %copy-done.2, f32[1,2]{1,0:T(1,128)S(1)} %bitcast.1, bf16[128,2048]{1,0:T(8,128)(2,1)S(1)} %copy-done.3), custom_call_target="tpu_custom_call" | custom-call | tf_op jit(solution)/shard_map/layer/pallas_call | solution.py:440
  75.2 0.7 copy.8
Async XLA Ops:
  0.0 0.7 copy-start.5
  0.7 1.0 %copy-start = (bf16[2048,128]{1,0:T(8,128)(2,1)S(1)}, bf16[2048,128]{1,0:T(8,128)(2,1)}, u32[]{:S(2)}) copy-start(bf16[2048,128]{1,0:T(8,128)(2,1)} %wq_hbm.1) | copy-start | bytes 1572868
  1.7 1.0 %copy-start.1 = (bf16[2048,128]{1,0:T(8,128)(2,1)S(1)}, bf16[2048,128]{1,0:T(8,128)(2,1)}, u32[]{:S(2)}) copy-start(bf16[2048,128]{1,0:T(8,128)(2,1)} %wk_hbm.1) | copy-start | bytes 1572868
  2.7 1.0 %copy-start.2 = (bf16[2048,128]{1,0:T(8,128)(2,1)S(1)}, bf16[2048,128]{1,0:T(8,128)(2,1)}, u32[]{:S(2)}) copy-start(bf16[2048,128]{1,0:T(8,128)(2,1)} %wv_hbm.1) | copy-start | bytes 1572868
  3.8 1.0 %copy-start.3 = (bf16[128,2048]{1,0:T(8,128)(2,1)S(1)}, bf16[128,2048]{1,0:T(8,128)(2,1)}, u32[]{:S(2)}) copy-start(bf16[128,2048]{1,0:T(8,128)(2,1)} %wo_hbm.1) | copy-start | bytes 1572868
  4.8 0.9 %copy-start.4 = (bf16[64,2048]{1,0:T(8,128)(2,1)S(1)}, bf16[64,2048]{1,0:T(8,128)(2,1)}, u32[]{:S(2)}) copy-start(bf16[64,2048]{1,0:T(8,128)(2,1)} %tok_hbm.1) | copy-start | bytes 786436
